TPU v7x, 32 devices: a whole 2x2x4 slice. The times are simulated.
32 devices in a mesh: grp: 2 (over y), sp: 4 (over z), tp: 4 (over x, core).
Axes of the slice: x: 2, y: 2, z: 4, core: 2. Of those that a mesh axis runs over, the one named last changes fastest.
Arguments:
- residual: bfloat16 [4096, 2048], P(('grp', 'sp', 'tp')), parts along dimension 0, may hold values from -6 to 6
- state_input: bfloat16 [4096, 1024], P(('grp', 'sp'), 'tp'), parts along dimension 0, may hold values from -6 to 6
- gate_input: bfloat16 [4096, 2048], P(('grp', 'sp'), 'tp'), parts along dimension 0, may hold values from -6 to 6
- decay_real: float32 [64, 64], P('tp'), may hold values from -0.2 to 0, as said below
- frequency: float32 [64, 64], P('tp'), as said below
- log_step: float32 [64], P('tp'), as said below
- drive_real: float32 [64, 64, 16], P('tp'), may hold values from -1 to 1
- drive_imag: float32 [64, 64, 16], P('tp'), may hold values from -1 to 1
- read_real: float32 [64, 16, 64], P('tp'), may hold values from -0.75 to 0.75
- read_imag: float32 [64, 16, 64], P('tp'), may hold values from -0.75 to 0.75
- skip_gain: float32 [1024], P('tp'), may hold values from -4 to 4
- value_weight: bfloat16 [1024, 2048], P(None, 'tp'), may hold values from -0.1875 to 0.1875
- glu_weight: bfloat16 [1024, 2048], P(None, 'tp'), may hold values from -0.1875 to 0.1875
- mix_weight: bfloat16 [2048, 2048], P('tp'), may hold values from -0.125 to 0.125
- norm_gain: float32 [2048], replicated, may hold values from 0.1 to 1.9
- mlp_gate: bfloat16 [2048, 3072], P('sp', 'tp'), may hold values from -0.125 to 0.125
- mlp_up: bfloat16 [2048, 3072], P('sp', 'tp'), may hold values from -0.125 to 0.125
- mlp_down: bfloat16 [3072, 2048], P('tp', 'sp'), may hold values from -0.109375 to 0.109375
Outputs:
- result: bfloat16 [4096, 2048], P(('grp', 'sp', 'tp')), parts along dimension 0
There are 2 independent parts, one for each index of `grp`. A program takes and returns all parts, laid end to end along the dimension named above; an argument that names none is the same for every part. Nothing has to cross between parts.
Inputs may be any that keep to these rules, and one draw needn't show every extreme that they name: `decay_real`: negative in every entry. `frequency`: never zero: its magnitude times exp(log_step) of its group lies between 0.05 and 0.5. Every group's time step exp(log_step) is at most one.
All inputs are finite; a program needn't handle non-finite values.
Results may differ from a plain program's by a relative error of at most 0.012.
Values may be sent and summed in bfloat16 or wider, within the bound.
A program may use at most 128 MiB of HBM per device.

v0:
```python
import functools
import jax
import jax.numpy as jnp
from jax import lax
from jax.experimental import pallas as pl
from jax.experimental.pallas import tpu as pltpu
from jax.sharding import PartitionSpec as P

BF = jnp.bfloat16
F32 = jnp.float32
ROWS8 = 8

HIGH = lax.Precision.HIGHEST
EPSILON = 1e-06


def carried_in(value, axis, join, neutral):
    count, mine = (lax.axis_size(axis), lax.axis_index(axis))
    pieces = jax.tree.map(lambda part: lax.all_gather(part, axis), value)
    subtotal = jax.tree.map(
        lambda part, zero: jnp.full_like(part, 0) + jnp.asarray(zero, part.dtype), value, neutral
    )

    def step(position, subtotal):
        longer = join(subtotal, jax.tree.map(lambda part: part[position], pieces))
        return jax.tree.map(lambda new, old: jnp.where(position < mine, new, old), longer, subtotal)

    return lax.fori_loop(0, count - 1, step, subtotal)


def discretize(decay_real, frequency, log_step, drive_real, drive_imag):
    step = jnp.exp(log_step)[:, None]
    magnitude = jnp.exp(decay_real * step)
    turned = frequency * step
    bar_real = magnitude * jnp.cos(turned)
    bar_imag = magnitude * jnp.sin(turned)
    modulus = decay_real * decay_real + frequency * frequency
    ratio_real = ((bar_real - 1.0) * decay_real + bar_imag * frequency) / modulus
    ratio_imag = (bar_imag * decay_real - (bar_real - 1.0) * frequency) / modulus
    in_real = ratio_real[..., None] * drive_real - ratio_imag[..., None] * drive_imag
    in_imag = ratio_real[..., None] * drive_imag + ratio_imag[..., None] * drive_real
    return (bar_real, bar_imag, in_real, in_imag)


def combine(earlier, later):
    real_one, imag_one, state_real_one, state_imag_one = earlier
    real_two, imag_two, state_real_two, state_imag_two = later
    return (
        real_one * real_two - imag_one * imag_two,
        real_one * imag_two + imag_one * real_two,
        real_two * state_real_one - imag_two * state_imag_one + state_real_two,
        real_two * state_imag_one + imag_two * state_real_one + state_imag_two,
    )


def powers(log_rate, angle_rate, count):
    return (
        jnp.exp(log_rate * count) * jnp.cos(angle_rate * count),
        jnp.exp(log_rate * count) * jnp.sin(angle_rate * count),
    )


def block_states(flat_inputs, decay_real, frequency, log_step, in_real, in_imag):
    rows = flat_inputs.shape[0]
    groups, states, width = in_real.shape
    flat = groups * states
    eye = jnp.eye(groups, dtype=jnp.float32)
    wide_real = jnp.einsum("gph,gk->ghkp", in_real, eye).reshape(groups * width, flat)
    wide_imag = jnp.einsum("gph,gk->ghkp", in_imag, eye).reshape(groups * width, flat)
    state_real = jnp.dot(flat_inputs, wide_real, precision=HIGH)
    state_imag = jnp.dot(flat_inputs, wide_imag, precision=HIGH)
    step = jnp.exp(log_step)[:, None]
    log_rate = (decay_real * step).reshape(1, flat)
    angle_rate = (frequency * step).reshape(1, flat)
    reach = 1
    while reach < rows:
        lift_real, lift_imag = powers(log_rate, angle_rate, float(reach))
        blank = jnp.zeros((reach, flat), jnp.float32)
        moved_real = jnp.concatenate([blank, state_real[: rows - reach]], axis=0)
        moved_imag = jnp.concatenate([blank, state_imag[: rows - reach]], axis=0)
        state_real, state_imag = (
            state_real + lift_real * moved_real - lift_imag * moved_imag,
            state_imag + lift_real * moved_imag + lift_imag * moved_real,
        )
        reach = reach * 2
    counts = (lax.iota(jnp.int32, rows) + 1).astype(jnp.float32)[:, None]
    power_real, power_imag = powers(log_rate, angle_rate, counts)
    return (power_real, power_imag, state_real, state_imag)


def readout(state_real, state_imag, read_real, read_imag, flat_inputs, skip_gain):
    groups, width, states = read_real.shape
    eye = jnp.eye(groups, dtype=jnp.float32)
    wide_real = jnp.einsum("ghp,gk->gpkh", read_real, eye).reshape(groups * states, groups * width)
    wide_imag = jnp.einsum("ghp,gk->gpkh", read_imag, eye).reshape(groups * states, groups * width)
    output = jnp.dot(state_real, wide_real, precision=HIGH) - jnp.dot(
        state_imag, wide_imag, precision=HIGH
    )
    output = output + skip_gain * flat_inputs
    return jax.nn.gelu(output).astype(jnp.bfloat16)


def normalize(inner, norm_gain):
    scale = lax.rsqrt(jnp.mean(inner * inner, axis=-1, keepdims=True) + EPSILON)
    return (inner * scale * norm_gain).astype(jnp.bfloat16)


def shards(
    residual,
    state_input,
    gate_input,
    decay_real,
    frequency,
    log_step,
    drive_real,
    drive_imag,
    read_real,
    read_imag,
    skip_gain,
    value_weight,
    glu_weight,
    mix_weight,
    norm_gain,
    mlp_gate,
    mlp_up,
    mlp_down,
):
    bar_real, bar_imag, in_real, in_imag = discretize(
        decay_real, frequency, log_step, drive_real, drive_imag
    )
    flat_inputs = state_input.astype(jnp.float32)
    power_real, power_imag, local_real, local_imag = block_states(
        flat_inputs, decay_real, frequency, log_step, in_real, in_imag
    )
    ends = (power_real[-1], power_imag[-1], local_real[-1], local_imag[-1])
    ones = jnp.ones_like(ends[0])
    zeros = jnp.zeros_like(ends[0])
    incoming = carried_in(
        (ends[0], ends[1], ends[2], ends[3]), "sp", combine, (ones, zeros, zeros, zeros)
    )
    carry_real = incoming[2]
    carry_imag = incoming[3]
    state_real = local_real + power_real * carry_real - power_imag * carry_imag
    state_imag = local_imag + power_real * carry_imag + power_imag * carry_real
    acts = readout(state_real, state_imag, read_real, read_imag, flat_inputs, skip_gain)
    piece = lax.all_gather(acts, "tp", axis=1, tiled=True)
    value = jnp.dot(piece, value_weight, preferred_element_type=jnp.float32)
    gated = jnp.dot(piece, glu_weight, preferred_element_type=jnp.float32)
    mixed = (jax.nn.sigmoid(gate_input.astype(jnp.float32)) * value * jax.nn.sigmoid(gated)).astype(
        jnp.bfloat16
    )
    branch = lax.psum_scatter(
        jnp.dot(mixed, mix_weight, preferred_element_type=jnp.float32).astype(jnp.bfloat16),
        "tp",
        scatter_dimension=0,
        tiled=True,
    ).astype(jnp.float32)
    inner = residual.astype(jnp.float32) + branch
    normed = lax.all_gather(normalize(inner, norm_gain), "tp", axis=0, tiled=True)
    hidden_gate = jnp.dot(
        normed,
        lax.all_gather(mlp_gate, "sp", axis=0, tiled=True),
        preferred_element_type=jnp.float32,
    )
    hidden_up = jnp.dot(
        normed, lax.all_gather(mlp_up, "sp", axis=0, tiled=True), preferred_element_type=jnp.float32
    )
    hidden = (jax.nn.silu(hidden_gate) * hidden_up).astype(jnp.bfloat16)
    down = jnp.dot(
        hidden,
        lax.all_gather(mlp_down, "sp", axis=1, tiled=True),
        preferred_element_type=jnp.float32,
    )
    down_own = lax.psum_scatter(
        down.astype(jnp.bfloat16), "tp", scatter_dimension=0, tiled=True
    ).astype(jnp.float32)
    return (inner + 0.5 * down_own).astype(jnp.bfloat16)


def mm(a, b):
    return jnp.dot(a, b, preferred_element_type=F32)


def mm_t(a, b):
    return lax.dot_general(a, b, (((1,), (1,)), ((), ())), preferred_element_type=F32)


def split(x):
    high = x.astype(BF)
    return high, (x - high.astype(F32)).astype(BF)


def layer_kernel(
    n_sp,
    width,
    states,
    residual,
    u,
    gate_in,
    pow_real,
    pow_imag,
    in_real,
    in_imag,
    rd_real,
    rd_imag,
    skip,
    value_h,
    glu_h,
    mix_h,
    gain,
    gate_h,
    up_h,
    down_h,
    out,
    value_w,
    glu_w,
    mix_w,
    w_gate,
    w_up,
    w_down,
    wide,
    st_real,
    st_imag,
    masked,
    ends,
    acts,
    part,
    rx_pair,
    relay,
    rx_far,
    inner,
    normed,
    hidden,
    c_part,
    c_pair,
    c_relay,
    c_far,
    load_sem,
    end_send,
    end_recv,
    z_send,
    z_recv,
    y_send,
    y_recv,
    ag_send,
    ag_recv,
    rs_send,
    rs_recv,
    c_send,
    c_recv,
):
    g, s, t = lax.axis_index("grp"), lax.axis_index("sp"), lax.axis_index("tp")
    low, high_bit = t % 2, t // 2
    p = t + 1 - 2 * low
    q = t + 2 - 4 * high_bit
    far = 3 - t
    other = 1 - g
    rows, chans = u.shape
    flat = st_real.shape[1]
    own, depth = residual.shape
    k_loc = gate_h.shape[0]
    ff, d_loc = down_h.shape
    k_half, f_half = k_loc // 2, ff // 2

    barrier = pltpu.get_barrier_semaphore()
    pl.semaphore_signal(barrier, inc=1, device_id={"tp": p})
    pl.semaphore_signal(barrier, inc=1, device_id={"tp": q})
    pl.semaphore_signal(barrier, inc=1, device_id={"grp": other})

    @pl.loop(1, n_sp)
    def _(d):
        pl.semaphore_signal(barrier, inc=1, device_id={"sp": (s + d) % n_sp})

    def mine(ref, c, origin, half):
        if c < 2:
            return ref.at[pl.ds(pl.multiple_of(origin * k_loc + half * k_half, k_half), k_half), :]
        return ref.at[origin, pl.ds(pl.multiple_of(half * f_half, f_half), f_half), :]

    bufs = (w_gate, w_up, w_down)
    place = pl.ds(pl.multiple_of(s * k_loc, k_loc), k_loc)
    loads = [
        pltpu.make_async_copy(gate_h, w_gate.at[place, :], load_sem.at[0]),
        pltpu.make_async_copy(up_h, w_up.at[place, :], load_sem.at[1]),
        pltpu.make_async_copy(down_h, w_down.at[s], load_sem.at[2]),
        pltpu.make_async_copy(value_h, value_w, load_sem.at[3]),
        pltpu.make_async_copy(glu_h, glu_w, load_sem.at[4]),
        pltpu.make_async_copy(mix_h, mix_w, load_sem.at[5]),
    ]
    for load in loads:
        load.start()
    pl.semaphore_wait(barrier, 3 + n_sp - 1)

    def z_copy(side, c, k, origin, target):
        piece = mine(bufs[c], c, origin, g)
        return pltpu.make_async_remote_copy(
            src_ref=piece,
            dst_ref=piece,
            send_sem=z_send.at[side, c, k],
            recv_sem=z_recv.at[side, c, k],
            device_id={"sp": target},
        )

    def y_copy(side, c, k, origin, half):
        piece = mine(bufs[c], c, origin, half)
        return pltpu.make_async_remote_copy(
            src_ref=piece,
            dst_ref=piece,
            send_sem=y_send.at[side, c, k],
            recv_sem=y_recv.at[side, c, k],
            device_id={"grp": other},
        )

    right, left = (s + 1) % n_sp, (s + n_sp - 1) % n_sp
    has_right, has_left = s < n_sp - 1, s > 0

    for c in range(3):
        loads[c].wait()

        @pl.when(has_right)
        def _():
            z_copy(0, c, 1, s, right).start()

        @pl.when(has_left)
        def _():
            z_copy(1, c, 1, s, left).start()

    def onward(c, k):
        @pl.when(s >= k)
        def _():
            origin = (s + n_sp - k) % n_sp
            z_copy(0, c, k, origin, right).wait_recv()

            @pl.when(has_right)
            def _():
                z_copy(0, c, k + 1, origin, right).start()

            y_copy(0, c, k, origin, g).start()

        @pl.when(s + k < n_sp)
        def _():
            origin = (s + k) % n_sp
            z_copy(1, c, k, origin, left).wait_recv()

            @pl.when(has_left)
            def _():
                z_copy(1, c, k + 1, origin, left).start()

            y_copy(1, c, k, origin, g).start()

    def arrived(c):
        @pl.loop(1, n_sp)
        def _(k):
            @pl.when(s >= k)
            def _():
                y_copy(0, c, k, (s + n_sp - k) % n_sp, other).wait_recv()

            @pl.when(s + k < n_sp)
            def _():
                y_copy(1, c, k, (s + k) % n_sp, other).wait_recv()

    lanes = in_real.shape[1]
    row_group = lax.broadcasted_iota(jnp.int32, (chans, lanes), 0) // width
    lane = lax.broadcasted_iota(jnp.int32, (chans, lanes), 1)
    for i, ref in enumerate((in_real, in_imag, rd_real, rd_imag)):
        value = ref[...]
        for tile in range(flat // lanes):
            kept = jnp.where(row_group == (lane + tile * lanes) // states, value, 0.0)
            big, small = split(kept)
            at = slice(tile * lanes, (tile + 1) * lanes)
            wide[2 * i, :, at] = big
            wide[2 * i + 1, :, at] = small

    @pl.loop(0, rows // own)
    def _(b):
        at = pl.ds(pl.multiple_of(b * own, own), own)
        x = u[at, :]
        st_real[at, :] = mm(x, wide[0]) + mm(x, wide[1])
        st_imag[at, :] = mm(x, wide[2]) + mm(x, wide[3])

    sub = lax.broadcasted_iota(jnp.int32, (ROWS8, flat), 0)
    for i, reach in enumerate((1, 2, 4)):
        masked[2 * i] = jnp.where(sub >= reach, pow_real[reach - 1 : reach, :], 0.0)
        masked[2 * i + 1] = jnp.where(sub >= reach, pow_imag[reach - 1 : reach, :], 0.0)

    def scan_step(b, carry):
        c_re, c_im = carry
        at = pl.ds(pl.multiple_of(b * ROWS8, ROWS8), ROWS8)
        x_re, x_im = st_real[at, :], st_imag[at, :]
        for i, reach in enumerate((1, 2, 4)):
            m_re, m_im = pltpu.roll(x_re, reach, 0), pltpu.roll(x_im, reach, 0)
            a_re, a_im = masked[2 * i], masked[2 * i + 1]
            x_re, x_im = x_re + a_re * m_re - a_im * m_im, x_im + a_re * m_im + a_im * m_re
        p_re, p_im = pow_real[...], pow_imag[...]
        x_re, x_im = x_re + p_re * c_re - p_im * c_im, x_im + p_re * c_im + p_im * c_re
        st_real[at, :] = x_re
        st_imag[at, :] = x_im
        return x_re[ROWS8 - 1 :, :], x_im[ROWS8 - 1 :, :]

    zero = jnp.zeros((1, flat), F32)
    end_re, end_im = lax.fori_loop(0, rows // ROWS8, scan_step, (zero, zero))
    ends[s, 0:1, :] = end_re
    ends[s, 1:2, :] = end_im

    def end_copy(target, origin):
        return pltpu.make_async_remote_copy(
            src_ref=ends.at[origin],
            dst_ref=ends.at[origin],
            send_sem=end_send.at[target],
            recv_sem=end_recv.at[origin],
            device_id={"sp": target},
        )

    @pl.loop(1, n_sp)
    def _(d):
        end_copy((s + d) % n_sp, s).start()

    onward(0, 1)
    last_re, last_im = pow_real[ROWS8 - 1 :, :], pow_imag[ROWS8 - 1 :, :]
    long_re, long_im = last_re, last_im
    reach = ROWS8
    while reach < rows:
        long_re, long_im = long_re * long_re - long_im * long_im, 2.0 * long_re * long_im
        reach *= 2

    @pl.loop(1, n_sp)
    def _(d):
        end_copy((s + d) % n_sp, (s + d) % n_sp).wait_recv()

    def carry_step(j, carry):
        c_re, c_im = carry
        e_re, e_im = ends[j, 0:1, :], ends[j, 1:2, :]
        n_re = long_re * c_re - long_im * c_im + e_re
        n_im = long_re * c_im + long_im * c_re + e_im
        return jnp.where(j < s, n_re, c_re), jnp.where(j < s, n_im, c_im)

    carry = lax.fori_loop(0, n_sp - 1, carry_step, (zero, zero))

    def lift(b, carry):
        c_re, c_im = carry
        at = pl.ds(pl.multiple_of(b * ROWS8, ROWS8), ROWS8)
        p_re, p_im = pow_real[...], pow_imag[...]
        st_real[at, :] = st_real[at, :] + p_re * c_re - p_im * c_im
        st_imag[at, :] = st_imag[at, :] + p_re * c_im + p_im * c_re
        return last_re * c_re - last_im * c_im, last_re * c_im + last_im * c_re

    lax.fori_loop(0, rows // ROWS8, lift, carry)

    @pl.loop(0, rows // own)
    def _(b):
        at = pl.ds(pl.multiple_of(b * own, own), own)
        high, small = split(st_real[at, :])
        y = mm_t(high, wide[4]) + mm_t(small, wide[4]) + mm_t(high, wide[5])
        high, small = split(st_imag[at, :])
        y = y - (mm_t(high, wide[6]) + mm_t(small, wide[6]) + mm_t(high, wide[7]))
        y = y + skip[...] * u[at, :].astype(F32)
        acts[t, at, :] = jax.nn.gelu(y).astype(BF)

    def gather_tp(buf, lane_no, between):
        def copy(slot, kind, target):
            return pltpu.make_async_remote_copy(
                src_ref=buf.at[slot],
                dst_ref=buf.at[slot],
                send_sem=ag_send.at[lane_no, kind],
                recv_sem=ag_recv.at[lane_no, kind],
                device_id={"tp": target},
            )

        sent = [copy(t, 0, q), copy(t, 1, p)]
        for item in sent:
            item.start()
        between()
        copy(q, 0, q).wait_recv()
        relayed = copy(q, 2, p)
        relayed.start()
        copy(p, 1, p).wait_recv()
        copy(far, 2, p).wait_recv()
        return sent + [relayed]

    def scatter_tp(lane_no, block, middle, between):
        def pair(index):
            return pltpu.make_async_remote_copy(
                src_ref=part.at[lane_no, (far, p)[index]],
                dst_ref=rx_pair.at[lane_no, index],
                send_sem=rs_send.at[lane_no, index],
                recv_sem=rs_recv.at[lane_no, index],
                device_id={"tp": p},
            )

        across = pltpu.make_async_remote_copy(
            src_ref=relay.at[lane_no],
            dst_ref=rx_far.at[lane_no],
            send_sem=rs_send.at[lane_no, 2],
            recv_sem=rs_recv.at[lane_no, 2],
            device_id={"tp": q},
        )
        pairs = [pair(0), pair(1)]
        block(far)
        pairs[0].start()
        block(p)
        pairs[1].start()
        block(q)
        middle()
        pairs[0].wait_recv()
        relay[lane_no] = (part[lane_no, q].astype(F32) + rx_pair[lane_no, 0].astype(F32)).astype(BF)
        across.start()
        block(t)
        between()
        pairs[1].wait_recv()
        across.wait_recv()
        return pairs + [across]

    def total(lane_no):
        near = part[lane_no, t].astype(F32) + rx_pair[lane_no, 1].astype(F32)
        return near + rx_far[lane_no].astype(F32)

    def first_forward():
        onward(1, 1)

    pending = gather_tp(acts, 0, first_forward)
    for load in loads[3:]:
        load.wait()
    n_tp = acts.shape[0]

    def mix_block(r):
        at = pl.ds(pl.multiple_of(r * own, own), own)
        value = jnp.zeros((own, value_w.shape[1]), F32)
        gated = value
        for j in range(n_tp):
            a = acts[j, at, :]
            value = value + mm(a, value_w[j * chans : (j + 1) * chans, :])
            gated = gated + mm(a, glu_w[j * chans : (j + 1) * chans, :])
        mixed = jax.nn.sigmoid(gate_in[at, :].astype(F32)) * value * jax.nn.sigmoid(gated)
        part[0, r] = mm(mixed.astype(BF), mix_w[...]).astype(BF)

    def third_forward():
        if n_sp > 2:
            onward(0, 2)

    pending += scatter_tp(0, mix_block, lambda: onward(2, 1), third_forward)
    inner[...] = residual[...].astype(F32) + total(0)
    x = inner[...]
    scale = lax.rsqrt(jnp.mean(x * x, axis=-1, keepdims=True) + EPSILON)
    normed[t] = (x * scale * gain[...]).astype(BF)

    def second_forward():
        if n_sp > 2:
            onward(1, 2)

    pending += gather_tp(normed, 1, second_forward)
    if n_sp > 2:
        onward(2, 2)

    @pl.loop(3, n_sp)
    def _(k):
        onward(0, k)
        onward(1, k)
        onward(2, k)

    arrived(0)
    arrived(1)

    @pl.loop(0, n_tp)
    def _(r):
        x = normed[r]
        hidden[r] = (jax.nn.silu(mm(x, w_gate[...])) * mm(x, w_up[...])).astype(BF)

    def col_pair(o, index):
        return pltpu.make_async_remote_copy(
            src_ref=c_part.at[o, (far, p)[index]],
            dst_ref=c_pair.at[o, index],
            send_sem=c_send.at[o, index],
            recv_sem=c_recv.at[o, index],
            device_id={"tp": p},
        )

    def col_far(o):
        return pltpu.make_async_remote_copy(
            src_ref=c_relay.at[o],
            dst_ref=c_far.at[o],
            send_sem=c_send.at[o, 2],
            recv_sem=c_recv.at[o, 2],
            device_id={"tp": q},
        )

    def column(o):
        weight = w_down.at[o]
        c_part[o, far] = mm(hidden[far], weight[...]).astype(BF)
        col_pair(o, 0).start()
        c_part[o, q] = mm(hidden[q], weight[...]).astype(BF)
        c_part[o, p] = mm(hidden[p], weight[...]).astype(BF)
        col_pair(o, 1).start()
        col_pair(o, 0).wait_recv()
        c_relay[o] = (c_part[o, q].astype(F32) + c_pair[o, 0].astype(F32)).astype(BF)
        col_far(o).start()
        c_part[o, t] = mm(hidden[t], weight[...]).astype(BF)

    column(s)

    @pl.loop(1, n_sp)
    def _(k):
        @pl.when(s >= k)
        def _():
            origin = (s + n_sp - k) % n_sp
            y_copy(0, 2, k, origin, other).wait_recv()
            column(origin)

        @pl.when(s + k < n_sp)
        def _():
            origin = (s + k) % n_sp
            y_copy(1, 2, k, origin, other).wait_recv()
            column(origin)

    for o in range(n_sp):
        col_pair(o, 1).wait_recv()
        col_far(o).wait_recv()
        near = c_part[o, t].astype(F32) + c_pair[o, 1].astype(F32)
        at = slice(o * d_loc, (o + 1) * d_loc)
        out[:, at] = (inner[:, at] + 0.5 * (near + c_far[o].astype(F32))).astype(BF)

    @pl.loop(0, n_sp)
    def _(o):
        col_pair(o, 0).wait_send()
        col_pair(o, 1).wait_send()
        col_far(o).wait_send()

    for item in pending:
        item.wait_send()

    @pl.loop(1, n_sp)
    def _(d):
        end_copy((s + d) % n_sp, s).wait_send()

    @pl.loop(1, n_sp)
    def _(k):
        for c in range(3):

            @pl.when(jnp.logical_and(has_right, s >= k - 1))
            def _():
                z_copy(0, c, k, (s + n_sp + 1 - k) % n_sp, right).wait_send()

            @pl.when(jnp.logical_and(has_left, s + k - 1 < n_sp))
            def _():
                z_copy(1, c, k, (s + k - 1) % n_sp, left).wait_send()

            @pl.when(s >= k)
            def _():
                y_copy(0, c, k, (s + n_sp - k) % n_sp, g).wait_send()

            @pl.when(s + k < n_sp)
            def _():
                y_copy(1, c, k, (s + k) % n_sp, g).wait_send()


def fused(
    residual,
    state_input,
    gate_input,
    decay_real,
    frequency,
    log_step,
    drive_real,
    drive_imag,
    read_real,
    read_imag,
    skip_gain,
    value_weight,
    glu_weight,
    mix_weight,
    norm_gain,
    mlp_gate,
    mlp_up,
    mlp_down,
):
    n_sp, n_tp = lax.axis_size("sp"), lax.axis_size("tp")
    groups, states, width = drive_real.shape
    flat, chans = groups * states, groups * width
    rows = state_input.shape[0]
    own, depth = residual.shape
    ff, d_loc = mlp_down.shape
    cols = value_weight.shape[1]
    _, _, in_real, in_imag = discretize(decay_real, frequency, log_step, drive_real, drive_imag)
    times = max(1, 128 // states)

    def tiled(x):
        return jnp.concatenate([x.reshape(chans, states)] * times, axis=1)

    step = jnp.exp(log_step)[:, None]
    counts = (lax.iota(jnp.int32, ROWS8) + 1).astype(F32)[:, None]
    pow_real, pow_imag = powers(
        (decay_real * step).reshape(1, flat), (frequency * step).reshape(1, flat), counts
    )
    vmem = pl.BlockSpec(memory_space=pltpu.VMEM)
    hbm = pl.BlockSpec(memory_space=pl.ANY)
    dma = pltpu.SemaphoreType.DMA
    return pl.pallas_call(
        functools.partial(layer_kernel, n_sp, width, states),
        out_shape=jax.ShapeDtypeStruct((own, depth), BF),
        in_specs=[vmem] * 10 + [hbm] * 3 + [vmem] + [hbm] * 3,
        out_specs=vmem,
        scratch_shapes=[
            pltpu.VMEM(value_weight.shape, BF),
            pltpu.VMEM(glu_weight.shape, BF),
            pltpu.VMEM(mix_weight.shape, BF),
            pltpu.VMEM((n_sp * mlp_gate.shape[0], ff), BF),
            pltpu.VMEM((n_sp * mlp_gate.shape[0], ff), BF),
            pltpu.VMEM((n_sp, ff, d_loc), BF),
            pltpu.VMEM((8, chans, flat), BF),
            pltpu.VMEM((rows, flat), F32),
            pltpu.VMEM((rows, flat), F32),
            pltpu.VMEM((6, ROWS8, flat), F32),
            pltpu.VMEM((n_sp, ROWS8, flat), F32),
            pltpu.VMEM((n_tp, rows, chans), BF),
            pltpu.VMEM((1, n_tp, own, depth), BF),
            pltpu.VMEM((1, 2, own, depth), BF),
            pltpu.VMEM((1, own, depth), BF),
            pltpu.VMEM((1, own, depth), BF),
            pltpu.VMEM((own, depth), F32),
            pltpu.VMEM((n_tp, own, depth), BF),
            pltpu.VMEM((n_tp, own, ff), BF),
            pltpu.VMEM((n_sp, n_tp, own, d_loc), BF),
            pltpu.VMEM((n_sp, 2, own, d_loc), BF),
            pltpu.VMEM((n_sp, own, d_loc), BF),
            pltpu.VMEM((n_sp, own, d_loc), BF),
            dma((6,)),
            dma((n_sp,)),
            dma((n_sp,)),
            dma((2, 3, n_sp)),
            dma((2, 3, n_sp)),
            dma((2, 3, n_sp)),
            dma((2, 3, n_sp)),
            dma((2, 3)),
            dma((2, 3)),
            dma((1, 3)),
            dma((1, 3)),
            dma((n_sp, 3)),
            dma((n_sp, 3)),
        ],
        compiler_params=pltpu.CompilerParams(
            collective_id=0, has_side_effects=True, vmem_limit_bytes=60 * 1024 * 1024
        ),
    )(
        residual,
        state_input,
        gate_input,
        pow_real,
        pow_imag,
        tiled(in_real.transpose(0, 2, 1)),
        tiled(in_imag.transpose(0, 2, 1)),
        tiled(read_real),
        tiled(read_imag),
        skip_gain[None, :],
        value_weight,
        glu_weight,
        mix_weight,
        norm_gain[None, :],
        mlp_gate,
        mlp_up,
        mlp_down,
    )


def solution(mesh):
    placed = (
        P(("grp", "sp", "tp"), None),
        P(("grp", "sp"), "tp"),
        P(("grp", "sp"), "tp"),
        P("tp", None),
        P("tp", None),
        P("tp"),
        P("tp", None, None),
        P("tp", None, None),
        P("tp", None, None),
        P("tp", None, None),
        P("tp"),
        P(None, "tp"),
        P(None, "tp"),
        P("tp", None),
        P(),
        P("sp", "tp"),
        P("sp", "tp"),
        P("tp", "sp"),
    )
    body = fused if (mesh.shape["tp"], mesh.shape["grp"]) == (4, 2) else shards
    return jax.shard_map(
        body, mesh=mesh, in_specs=placed, out_specs=P(("grp", "sp", "tp"), None), check_vma=False
    )
```

profile of v0, /device:TPU:0, one launch (start us, length us, event | category | flops | bytes accessed | tf_op | source)
XLA Modules:
  0.0 135.9 jit_solution(17434741035341808582)
XLA Ops:
  0.0 0.7 exp.11
  0.7 0.8 fusion.2
  1.5 0.1 mul.56
  1.6 0.1 mul.61
  1.6 0.8 fusion.1
  2.5 1.0 multiply_add_fusion
  3.5 0.8 pad_maximum_fusion
  4.3 1.9 %pad_maximum_fusion.2 = (f32[256,128]{1,0:T(8,128)}, f32[256,128]{1,0:T(8,128)}) fusion(f32[256,64]{1,0:T(8,128)} %bitcast.12, f32[256,64]{1,0:T(8,128)} %bitcast.13), kind=kLoop, calls=%fused_computation.2 | loop fusion | flops 65536 | bytes 393216 | tf_op jit(solution)/shard_map/concatenate | solution.py:685
  6.2 127.7 %shard_map.172 = bf16[128,2048]{1,0:T(8,128)(2,1)} custom-call(bf16[128,2048]{1,0:T(8,128)(2,1)} %residual.1, bf16[512,256]{1,0:T(8,128)(2,1)} %u.1, bf16[512,512]{1,0:T(8,128)(2,1)} %gate_in.1, f32[8,1024]{1,0:T(8,128)} %get-tuple-element.12.pow_real, f32[8,1024]{1,0:T(8,128)} %get-tuple-element.11.pow_imag, f32[256,128]{1,0:T(8,128)} %get-tuple-element.13.in_real, ...), custom_call_target="tpu_custom_call" | custom-call | tf_op jit(solution)/shard_map/pallas_call | solution.py:695
  134.0 1.9 %copy.20 = bf16[128,2048]{1,0:T(8,128)(2,1)} copy(bf16[128,2048]{1,0:T(8,128)(2,1)} %shard_map.172) | data formatting | bytes 1048576
  (1 shorter events, 0.0 us)
where the time goes:
time: 136 us
  Pallas kernels  128 us (94%)
  other arithmetic  5.44 us (4%)
  local copies, waits for them, and re-layouts  2.68 us (2%)
    pallas_call x1, Pallas kernels, fused(): pl.pallas_call(functools.partial(layer_kernel, n_sp, width, states), out_...  128 us
    concatenate x2, other arithmetic, tiled(): return jnp.concatenate([x.reshape(chans, states)] * times, axis=1)  2.76 us

commit v1 on v0

--- a/solution.py
+++ b/solution.py
@@ -9,6 +9,7 @@
 BF = jnp.bfloat16
 F32 = jnp.float32
 ROWS8 = 8
+PIECES = 2
 
 HIGH = lax.Precision.HIGHEST
 EPSILON = 1e-06
@@ -759,6 +760,577 @@
     )
 
 
+def quick_kernel(
+    n_sp,
+    width,
+    states,
+    residual,
+    u,
+    gate_in,
+    pow_real,
+    pow_imag,
+    in_real,
+    in_imag,
+    rd_real,
+    rd_imag,
+    skip,
+    value_h,
+    glu_h,
+    mix_h,
+    gain,
+    gate_h,
+    up_h,
+    down_h,
+    out,
+    value_w,
+    glu_w,
+    mix_w,
+    w_gate,
+    w_up,
+    w_down,
+    wide,
+    st_real,
+    st_imag,
+    masked,
+    ends,
+    acts,
+    part,
+    rx_pair,
+    relay,
+    rx_far,
+    inner,
+    normed,
+    hidden,
+    c_part,
+    c_pair,
+    c_relay,
+    c_far,
+    load_sem,
+    end_send,
+    end_recv,
+    z_send,
+    z_recv,
+    y_send,
+    y_recv,
+    ag_send,
+    ag_recv,
+    rs_send,
+    rs_recv,
+    c_send,
+    c_recv,
+):
+    g, s, t = lax.axis_index("grp"), lax.axis_index("sp"), lax.axis_index("tp")
+    low, high_bit = t % 2, t // 2
+    p = t + 1 - 2 * low
+    q = t + 2 - 4 * high_bit
+    far = 3 - t
+    other = 1 - g
+    rows, chans = u.shape
+    flat = st_real.shape[1]
+    own, depth = residual.shape
+    k_loc = gate_h.shape[0]
+    ff, d_loc = down_h.shape
+    k_half, f_half = k_loc // 2, ff // 2
+
+    barrier = pltpu.get_barrier_semaphore()
+    pl.semaphore_signal(barrier, inc=1, device_id={"tp": p})
+    pl.semaphore_signal(barrier, inc=1, device_id={"tp": q})
+    pl.semaphore_signal(barrier, inc=1, device_id={"grp": other})
+
+    @pl.loop(1, n_sp)
+    def _(d):
+        pl.semaphore_signal(barrier, inc=1, device_id={"sp": (s + d) % n_sp})
+
+    bufs = (w_gate, w_up, w_down)
+    place = pl.ds(pl.multiple_of(s * k_loc, k_loc), k_loc)
+    loads = [
+        pltpu.make_async_copy(gate_h, w_gate.at[place, :], load_sem.at[0]),
+        pltpu.make_async_copy(up_h, w_up.at[place, :], load_sem.at[1]),
+        pltpu.make_async_copy(down_h, w_down.at[s], load_sem.at[2]),
+        pltpu.make_async_copy(value_h, value_w, load_sem.at[3]),
+        pltpu.make_async_copy(glu_h, glu_w, load_sem.at[4]),
+        pltpu.make_async_copy(mix_h, mix_w, load_sem.at[5]),
+    ]
+    for load in loads:
+        load.start()
+    pl.semaphore_wait(barrier, 3 + n_sp - 1)
+
+    k_piece, d_piece = k_half // PIECES, d_loc // PIECES
+
+    def mine(c, i, origin, half):
+        if c < 2:
+            row = pl.multiple_of(origin * k_loc + half * k_half + i * k_piece, k_piece)
+            return bufs[c].at[pl.ds(row, k_piece), :]
+        row = pl.multiple_of(half * f_half, f_half)
+        return bufs[c].at[origin, pl.ds(row, f_half), pl.ds(i * d_piece, d_piece)]
+
+    def z_copy(side, c, i, k, origin, target):
+        piece = mine(c, i, origin, g)
+        return pltpu.make_async_remote_copy(
+            src_ref=piece,
+            dst_ref=piece,
+            send_sem=z_send.at[side, c, i, k],
+            recv_sem=z_recv.at[side, c, i, k],
+            device_id={"sp": target},
+        )
+
+    def y_copy(side, c, i, k, origin, half):
+        piece = mine(c, i, origin, half)
+        return pltpu.make_async_remote_copy(
+            src_ref=piece,
+            dst_ref=piece,
+            send_sem=y_send.at[side, c, i, k],
+            recv_sem=y_recv.at[side, c, i, k],
+            device_id={"grp": other},
+        )
+
+    def spots(behind, side):
+        here = behind if side == 0 else n_sp - 1 - behind
+        step = 1 if side == 0 else -1
+        return here, step, behind < n_sp - 1
+
+    def order(behind):
+        early = [(k, c, i) for k in range(1, behind + 1) for c in (0, 1) for i in range(PIECES)]
+        late = [(k, 2, i) for k in range(1, behind + 1) for i in range(PIECES)]
+        return early, late
+
+    def send_own(side, c, here, step):
+        for i in range(PIECES):
+            z_copy(side, c, i, 1, s, here + step).start()
+
+    def own_sends(c):
+        loads[c].wait()
+        for side in range(2):
+            for behind in range(n_sp - 1):
+                here, step, onward = spots(behind, side)
+                if c < 2 or behind == 0:
+                    pl.when(s == here)(functools.partial(send_own, side, c, here, step))
+
+    own_sends(0)
+
+    def pass_on(side, behind, number):
+        here, step, onward = spots(behind, side)
+        early, late = order(behind)
+        k, c, i = (early + late)[number]
+        origin = here - step * k
+        z_copy(side, c, i, k, origin, here).wait_recv()
+        if onward:
+            z_copy(side, c, i, k + 1, origin, here + step).start()
+        y_copy(side, c, i, k, origin, g).start()
+        if onward and number == len(early) - 1:
+            send_own(side, 2, here, step)
+
+    def advance(*numbers):
+        for number in numbers:
+            for side in range(2):
+                for behind in range(1, n_sp):
+                    here = spots(behind, side)[0]
+                    if number < 3 * PIECES * behind:
+                        pl.when(s == here)(functools.partial(pass_on, side, behind, number))
+
+    def landed(side, behind, kinds, ks):
+        here, step, _ = spots(behind, side)
+        for k in ks:
+            for c in kinds:
+                for i in range(PIECES):
+                    y_copy(side, c, i, k, here - step * k, other).wait_recv()
+
+    def finish_sends(side, behind):
+        here, step, onward = spots(behind, side)
+        for c in range(3):
+            for i in range(PIECES):
+                for k in range(1, behind + 1):
+                    y_copy(side, c, i, k, here - step * k, g).wait_send()
+                if onward:
+                    for k in range(1, behind + 2):
+                        z_copy(side, c, i, k, here - step * (k - 1), here + step).wait_send()
+
+    lanes = in_real.shape[1]
+    row_group = lax.broadcasted_iota(jnp.int32, (chans, lanes), 0) // width
+    lane = lax.broadcasted_iota(jnp.int32, (chans, lanes), 1)
+    for i, ref in enumerate((in_real, in_imag, rd_real, rd_imag)):
+        value = ref[...]
+        for tile in range(flat // lanes):
+            kept = jnp.where(row_group == (lane + tile * lanes) // states, value, 0.0)
+            big, small = split(kept)
+            at = slice(tile * lanes, (tile + 1) * lanes)
+            wide[2 * i, :, at] = big
+            wide[2 * i + 1, :, at] = small
+
+    @pl.loop(0, rows // own)
+    def _(b):
+        at = pl.ds(pl.multiple_of(b * own, own), own)
+        x = u[at, :]
+        st_real[at, :] = mm(x, wide[0]) + mm(x, wide[1])
+        st_imag[at, :] = mm(x, wide[2]) + mm(x, wide[3])
+
+    sub = lax.broadcasted_iota(jnp.int32, (ROWS8, flat), 0)
+    for i, reach in enumerate((1, 2, 4)):
+        masked[2 * i] = jnp.where(sub >= reach, pow_real[reach - 1 : reach, :], 0.0)
+        masked[2 * i + 1] = jnp.where(sub >= reach, pow_imag[reach - 1 : reach, :], 0.0)
+
+    def scan_step(b, carry):
+        c_re, c_im = carry
+        at = pl.ds(pl.multiple_of(b * ROWS8, ROWS8), ROWS8)
+        x_re, x_im = st_real[at, :], st_imag[at, :]
+        for i, reach in enumerate((1, 2, 4)):
+            m_re, m_im = pltpu.roll(x_re, reach, 0), pltpu.roll(x_im, reach, 0)
+            a_re, a_im = masked[2 * i], masked[2 * i + 1]
+            x_re, x_im = x_re + a_re * m_re - a_im * m_im, x_im + a_re * m_im + a_im * m_re
+        p_re, p_im = pow_real[...], pow_imag[...]
+        x_re, x_im = x_re + p_re * c_re - p_im * c_im, x_im + p_re * c_im + p_im * c_re
+        st_real[at, :] = x_re
+        st_imag[at, :] = x_im
+        return x_re[ROWS8 - 1 :, :], x_im[ROWS8 - 1 :, :]
+
+    zero = jnp.zeros((1, flat), F32)
+    end_re, end_im = lax.fori_loop(0, rows // ROWS8, scan_step, (zero, zero))
+    ends[s, :, :flat] = end_re
+    ends[s, :, flat:] = end_im
+
+    def end_copy(target, origin):
+        return pltpu.make_async_remote_copy(
+            src_ref=ends.at[origin],
+            dst_ref=ends.at[origin],
+            send_sem=end_send.at[target],
+            recv_sem=end_recv.at[origin],
+            device_id={"sp": target},
+        )
+
+    @pl.loop(1, n_sp)
+    def _(d):
+        end_copy((s + d) % n_sp, s).start()
+
+    own_sends(1)
+    own_sends(2)
+    advance(0)
+    last_re, last_im = pow_real[ROWS8 - 1 :, :], pow_imag[ROWS8 - 1 :, :]
+    long_re, long_im = last_re, last_im
+    reach = ROWS8
+    while reach < rows:
+        long_re, long_im = long_re * long_re - long_im * long_im, 2.0 * long_re * long_im
+        reach *= 2
+
+    @pl.loop(1, n_sp)
+    def _(d):
+        end_copy((s + d) % n_sp, (s + d) % n_sp).wait_recv()
+
+    def carry_step(j, carry):
+        c_re, c_im = carry
+        e_re, e_im = ends[j, :, :flat], ends[j, :, flat:]
+        n_re = long_re * c_re - long_im * c_im + e_re
+        n_im = long_re * c_im + long_im * c_re + e_im
+        return jnp.where(j < s, n_re, c_re), jnp.where(j < s, n_im, c_im)
+
+    carry = lax.fori_loop(0, n_sp - 1, carry_step, (zero, zero))
+
+    def lift(b, carry):
+        c_re, c_im = carry
+        at = pl.ds(pl.multiple_of(b * ROWS8, ROWS8), ROWS8)
+        p_re, p_im = pow_real[...], pow_imag[...]
+        st_real[at, :] = st_real[at, :] + p_re * c_re - p_im * c_im
+        st_imag[at, :] = st_imag[at, :] + p_re * c_im + p_im * c_re
+        return last_re * c_re - last_im * c_im, last_re * c_im + last_im * c_re
+
+    lax.fori_loop(0, rows // ROWS8, lift, carry)
+    advance(1)
+
+    @pl.loop(0, rows // own)
+    def _(b):
+        at = pl.ds(pl.multiple_of(b * own, own), own)
+        high, small = split(st_real[at, :])
+        y = mm_t(high, wide[4]) + mm_t(small, wide[4]) + mm_t(high, wide[5])
+        high, small = split(st_imag[at, :])
+        y = y - (mm_t(high, wide[6]) + mm_t(small, wide[6]) + mm_t(high, wide[7]))
+        y = y + skip[...] * u[at, :].astype(F32)
+        acts[t, at, :] = jax.nn.gelu(y).astype(BF)
+
+    def gather_tp(buf, lane_no, between, later):
+        def copy(slot, kind, target):
+            return pltpu.make_async_remote_copy(
+                src_ref=buf.at[slot],
+                dst_ref=buf.at[slot],
+                send_sem=ag_send.at[lane_no, kind],
+                recv_sem=ag_recv.at[lane_no, kind],
+                device_id={"tp": target},
+            )
+
+        sent = [copy(t, 0, q), copy(t, 1, p)]
+        for item in sent:
+            item.start()
+        between()
+        copy(q, 0, q).wait_recv()
+        relayed = copy(q, 2, p)
+        relayed.start()
+        later()
+        copy(p, 1, p).wait_recv()
+        copy(far, 2, p).wait_recv()
+        return sent + [relayed]
+
+    def scatter_tp(lane_no, block, middle, between):
+        def pair(index):
+            return pltpu.make_async_remote_copy(
+                src_ref=part.at[lane_no, (far, p)[index]],
+                dst_ref=rx_pair.at[lane_no, index],
+                send_sem=rs_send.at[lane_no, index],
+                recv_sem=rs_recv.at[lane_no, index],
+                device_id={"tp": p},
+            )
+
+        across = pltpu.make_async_remote_copy(
+            src_ref=relay.at[lane_no],
+            dst_ref=rx_far.at[lane_no],
+            send_sem=rs_send.at[lane_no, 2],
+            recv_sem=rs_recv.at[lane_no, 2],
+            device_id={"tp": q},
+        )
+        pairs = [pair(0), pair(1)]
+        block(far)
+        pairs[0].start()
+        block(p)
+        pairs[1].start()
+        block(q)
+        middle()
+        pairs[0].wait_recv()
+        relay[lane_no] = (part[lane_no, q].astype(F32) + rx_pair[lane_no, 0].astype(F32)).astype(BF)
+        across.start()
+        block(t)
+        between()
+        pairs[1].wait_recv()
+        across.wait_recv()
+        return pairs + [across]
+
+    def total(lane_no):
+        near = part[lane_no, t].astype(F32) + rx_pair[lane_no, 1].astype(F32)
+        return near + rx_far[lane_no].astype(F32)
+
+    pending = gather_tp(acts, 0, lambda: advance(2), lambda: advance(3))
+    for load in loads[3:]:
+        load.wait()
+    n_tp = acts.shape[0]
+
+    def mix_block(r):
+        at = pl.ds(pl.multiple_of(r * own, own), own)
+        value = jnp.zeros((own, value_w.shape[1]), F32)
+        gated = value
+        for j in range(n_tp):
+            a = acts[j, at, :]
+            value = value + mm(a, value_w[j * chans : (j + 1) * chans, :])
+            gated = gated + mm(a, glu_w[j * chans : (j + 1) * chans, :])
+        mixed = jax.nn.sigmoid(gate_in[at, :].astype(F32)) * value * jax.nn.sigmoid(gated)
+        part[0, r] = mm(mixed.astype(BF), mix_w[...]).astype(BF)
+
+    pending += scatter_tp(0, mix_block, lambda: advance(4), lambda: advance(5, 6, 7))
+    inner[...] = residual[...].astype(F32) + total(0)
+    x = inner[...]
+    scale = lax.rsqrt(jnp.mean(x * x, axis=-1, keepdims=True) + EPSILON)
+    normed[t] = (x * scale * gain[...]).astype(BF)
+
+    pending += gather_tp(normed, 1, lambda: advance(8, 9), lambda: advance(10))
+    advance(11, 12)
+    for side in range(2):
+        for behind in range(1, n_sp):
+            here = spots(behind, side)[0]
+            ready = functools.partial(landed, side, behind, (0, 1), range(1, behind + 1))
+            pl.when(s == here)(ready)
+
+    @pl.loop(0, n_tp)
+    def _(r):
+        x = normed[r]
+        hidden[r] = (jax.nn.silu(mm(x, w_gate[...])) * mm(x, w_up[...])).astype(BF)
+
+    def col_pair(o, h, index):
+        return pltpu.make_async_remote_copy(
+            src_ref=c_part.at[o, h, (far, p)[index]],
+            dst_ref=c_pair.at[o, h, index],
+            send_sem=c_send.at[o, h, index],
+            recv_sem=c_recv.at[o, h, index],
+            device_id={"tp": p},
+        )
+
+    def col_far(o, h):
+        return pltpu.make_async_remote_copy(
+            src_ref=c_relay.at[o, h],
+            dst_ref=c_far.at[o, h],
+            send_sem=c_send.at[o, h, 2],
+            recv_sem=c_recv.at[o, h, 2],
+            device_id={"tp": q},
+        )
+
+    def column(o):
+        for h in range(PIECES):
+            weight = w_down.at[o, :, h * d_piece : (h + 1) * d_piece]
+            for r, index in ((far, 0), (p, 1), (q, None), (t, None)):
+                c_part[o, h, r] = mm(hidden[r], weight[...]).astype(BF)
+                if index is not None:
+                    col_pair(o, h, index).start()
+        for h in range(PIECES):
+            col_pair(o, h, 0).wait_recv()
+            both = c_part[o, h, q].astype(F32) + c_pair[o, h, 0].astype(F32)
+            c_relay[o, h] = both.astype(BF)
+            col_far(o, h).start()
+
+    def settle(o):
+        for h in range(PIECES):
+            col_pair(o, h, 1).wait_recv()
+            col_far(o, h).wait_recv()
+            near = c_part[o, h, t].astype(F32) + c_pair[o, h, 1].astype(F32)
+            at = pl.ds(pl.multiple_of(o * d_loc + h * d_piece, d_piece), d_piece)
+            out[:, at] = (inner[:, at] + 0.5 * (near + c_far[o, h].astype(F32))).astype(BF)
+
+    def both_sides(k, work):
+        for side in range(2):
+            for behind in range(k, n_sp):
+                here, step, _ = spots(behind, side)
+                pl.when(s == here)(functools.partial(work, side, behind, k, here - step * k))
+
+    def next_column(side, behind, k, origin):
+        landed(side, behind, (2,), (k,))
+        column(origin)
+
+    def next_settle(side, behind, k, origin):
+        settle(origin)
+
+    column(s)
+    advance(13)
+    for k in range(1, n_sp):
+        upto = range(12 + 2 * k, min(12 + 2 * k + 2, 3 * PIECES * (n_sp - 1)))
+        advance(*upto)
+        both_sides(k, next_column)
+        if k == 1:
+            settle(s)
+        else:
+            both_sides(k - 1, next_settle)
+    both_sides(n_sp - 1, next_settle)
+
+    @pl.loop(0, n_sp)
+    def _(o):
+        for h in range(PIECES):
+            col_pair(o, h, 0).wait_send()
+            col_pair(o, h, 1).wait_send()
+            col_far(o, h).wait_send()
+
+    for item in pending:
+        item.wait_send()
+
+    @pl.loop(1, n_sp)
+    def _(d):
+        end_copy((s + d) % n_sp, s).wait_send()
+
+    for side in range(2):
+        for behind in range(n_sp):
+            here = spots(behind, side)[0]
+            pl.when(s == here)(functools.partial(finish_sends, side, behind))
+
+
+def quick(
+    residual,
+    state_input,
+    gate_input,
+    decay_real,
+    frequency,
+    log_step,
+    drive_real,
+    drive_imag,
+    read_real,
+    read_imag,
+    skip_gain,
+    value_weight,
+    glu_weight,
+    mix_weight,
+    norm_gain,
+    mlp_gate,
+    mlp_up,
+    mlp_down,
+):
+    n_sp, n_tp = lax.axis_size("sp"), lax.axis_size("tp")
+    groups, states, width = drive_real.shape
+    flat, chans = groups * states, groups * width
+    rows = state_input.shape[0]
+    own, depth = residual.shape
+    ff, d_loc = mlp_down.shape
+    cols = value_weight.shape[1]
+    _, _, in_real, in_imag = discretize(decay_real, frequency, log_step, drive_real, drive_imag)
+    times = max(1, 128 // states)
+
+    def tiled(x):
+        return jnp.concatenate([x.reshape(chans, states)] * times, axis=1)
+
+    step = jnp.exp(log_step)[:, None]
+    counts = (lax.iota(jnp.int32, ROWS8) + 1).astype(F32)[:, None]
+    pow_real, pow_imag = powers(
+        (decay_real * step).reshape(1, flat), (frequency * step).reshape(1, flat), counts
+    )
+    vmem = pl.BlockSpec(memory_space=pltpu.VMEM)
+    hbm = pl.BlockSpec(memory_space=pl.ANY)
+    dma = pltpu.SemaphoreType.DMA
+    return pl.pallas_call(
+        functools.partial(quick_kernel, n_sp, width, states),
+        out_shape=jax.ShapeDtypeStruct((own, depth), BF),
+        in_specs=[vmem] * 10 + [hbm] * 3 + [vmem] + [hbm] * 3,
+        out_specs=vmem,
+        scratch_shapes=[
+            pltpu.VMEM(value_weight.shape, BF),
+            pltpu.VMEM(glu_weight.shape, BF),
+            pltpu.VMEM(mix_weight.shape, BF),
+            pltpu.VMEM((n_sp * mlp_gate.shape[0], ff), BF),
+            pltpu.VMEM((n_sp * mlp_gate.shape[0], ff), BF),
+            pltpu.VMEM((n_sp, ff, d_loc), BF),
+            pltpu.VMEM((8, chans, flat), BF),
+            pltpu.VMEM((rows, flat), F32),
+            pltpu.VMEM((rows, flat), F32),
+            pltpu.VMEM((6, ROWS8, flat), F32),
+            pltpu.VMEM((n_sp, 1, 2 * flat), F32),
+            pltpu.VMEM((n_tp, rows, chans), BF),
+            pltpu.VMEM((1, n_tp, own, depth), BF),
+            pltpu.VMEM((1, 2, own, depth), BF),
+            pltpu.VMEM((1, own, depth), BF),
+            pltpu.VMEM((1, own, depth), BF),
+            pltpu.VMEM((own, depth), F32),
+            pltpu.VMEM((n_tp, own, depth), BF),
+            pltpu.VMEM((n_tp, own, ff), BF),
+            pltpu.VMEM((n_sp, PIECES, n_tp, own, d_loc // PIECES), BF),
+            pltpu.VMEM((n_sp, PIECES, 2, own, d_loc // PIECES), BF),
+            pltpu.VMEM((n_sp, PIECES, own, d_loc // PIECES), BF),
+            pltpu.VMEM((n_sp, PIECES, own, d_loc // PIECES), BF),
+            dma((6,)),
+            dma((n_sp,)),
+            dma((n_sp,)),
+            dma((2, 3, PIECES, n_sp)),
+            dma((2, 3, PIECES, n_sp)),
+            dma((2, 3, PIECES, n_sp)),
+            dma((2, 3, PIECES, n_sp)),
+            dma((2, 3)),
+            dma((2, 3)),
+            dma((1, 3)),
+            dma((1, 3)),
+            dma((n_sp, PIECES, 3)),
+            dma((n_sp, PIECES, 3)),
+        ],
+        compiler_params=pltpu.CompilerParams(
+            collective_id=0, has_side_effects=True, vmem_limit_bytes=60 * 1024 * 1024
+        ),
+    )(
+        residual,
+        state_input,
+        gate_input,
+        pow_real,
+        pow_imag,
+        tiled(in_real.transpose(0, 2, 1)),
+        tiled(in_imag.transpose(0, 2, 1)),
+        tiled(read_real),
+        tiled(read_imag),
+        skip_gain[None, :],
+        value_weight,
+        glu_weight,
+        mix_weight,
+        norm_gain[None, :],
+        mlp_gate,
+        mlp_up,
+        mlp_down,
+    )
+
+
 def solution(mesh):
     placed = (
         P(("grp", "sp", "tp"), None),
@@ -780,7 +1352,9 @@
         P("sp", "tp"),
         P("tp", "sp"),
     )
-    body = fused if (mesh.shape["tp"], mesh.shape["grp"]) == (4, 2) else shards
+    body = shards
+    if (mesh.shape["tp"], mesh.shape["grp"]) == (4, 2):
+        body = quick if mesh.shape["sp"] == 4 else fused
     return jax.shard_map(
         body, mesh=mesh, in_specs=placed, out_specs=P(("grp", "sp", "tp"), None), check_vma=False
     )

time: 136 us -> 119 us (0.88)
  Pallas kernels: 128 us -> 110 us
    pallas_call x1, Pallas kernels: 128 us -> 110 us  [quick(): pl.pallas_call(functools.partial(quick_kernel, n_sp, width, states), out_...]
where the time goes in v1:
time: 119 us; the launch traced here: 118 us
  Pallas kernels  110 us (92%)
  other arithmetic  5.44 us (5%)
  local copies, waits for them, and re-layouts  2.68 us (2%)
    pallas_call x1, Pallas kernels, quick(): pl.pallas_call(functools.partial(quick_kernel, n_sp, width, states), out_...  110 us
    concatenate x2, other arithmetic, tiled(): return jnp.concatenate([x.reshape(chans, states)] * times, axis=1)  2.76 us

profile of v1, /device:TPU:0, one launch (start us, length us, event | category | flops | bytes accessed | tf_op | source)
XLA Modules:
  0.0 118.2 jit_solution(16918384353874172934)
XLA Ops:
  0.0 0.7 exp.11
  0.7 0.8 fusion.2
  1.5 0.1 mul.56
  1.6 0.1 mul.61
  1.6 0.8 fusion.1
  2.5 1.0 multiply_add_fusion
  3.5 0.8 pad_maximum_fusion
  4.3 1.9 %pad_maximum_fusion.2 = (f32[256,128]{1,0:T(8,128)}, f32[256,128]{1,0:T(8,128)}) fusion(f32[256,64]{1,0:T(8,128)} %bitcast.12, f32[256,64]{1,0:T(8,128)} %bitcast.13), kind=kLoop, calls=%fused_computation.2 | loop fusion | flops 65536 | bytes 393216 | tf_op jit(solution)/shard_map/concatenate | solution.py:1257
  6.2 110.1 %shard_map.172 = bf16[128,2048]{1,0:T(8,128)(2,1)} custom-call(bf16[128,2048]{1,0:T(8,128)(2,1)} %residual.1, bf16[512,256]{1,0:T(8,128)(2,1)} %u.1, bf16[512,512]{1,0:T(8,128)(2,1)} %gate_in.1, f32[8,1024]{1,0:T(8,128)} %get-tuple-element.12.pow_real, f32[8,1024]{1,0:T(8,128)} %get-tuple-element.11.pow_imag, f32[256,128]{1,0:T(8,128)} %get-tuple-element.13.in_real, ...), custom_call_target="tpu_custom_call" | custom-call | tf_op jit(solution)/shard_map/pallas_call | solution.py:1267
  116.3 1.9 %copy.20 = bf16[128,2048]{1,0:T(8,128)(2,1)} copy(bf16[128,2048]{1,0:T(8,128)(2,1)} %shard_map.172) | data formatting | bytes 1048576
  (1 shorter events, 0.0 us)

commit v2 on v0

--- a/solution.py
+++ b/solution.py
@@ -9,6 +9,8 @@
 BF = jnp.bfloat16
 F32 = jnp.float32
 ROWS8 = 8
+PIECES = 4
+HALVES = 2
 
 HIGH = lax.Precision.HIGHEST
 EPSILON = 1e-06
@@ -759,6 +761,702 @@
     )
 
 
+def quick_kernel(
+    n_sp,
+    width,
+    states,
+    residual_h,
+    u_h,
+    gate_in_h,
+    decay_h,
+    freq_h,
+    step_h,
+    drive_re_h,
+    drive_im_h,
+    read_re_h,
+    read_im_h,
+    skip_h,
+    value_h,
+    glu_h,
+    mix_h,
+    gain_h,
+    gate_h,
+    up_h,
+    down_h,
+    out,
+    residual,
+    u,
+    gate_in,
+    decay,
+    freq,
+    log_step,
+    drive_re,
+    drive_im,
+    read_re,
+    read_im,
+    skip,
+    value_w,
+    glu_w,
+    mix_w,
+    gain,
+    w_gate,
+    w_up,
+    w_down,
+    wide,
+    pow_real,
+    pow_imag,
+    ratio,
+    st_real,
+    st_imag,
+    masked,
+    ends,
+    acts,
+    part,
+    rx_pair,
+    relay,
+    rx_far,
+    inner,
+    normed,
+    hidden,
+    c_part,
+    c_in,
+    c_relay,
+    load_sem,
+    end_send,
+    end_recv,
+    z_send,
+    z_recv,
+    y_send,
+    y_recv,
+    y_late,
+    z_more,
+    ag_send,
+    ag_recv,
+    rs_send,
+    rs_recv,
+    c_send,
+    c_recv,
+):
+    g, s, t = lax.axis_index("grp"), lax.axis_index("sp"), lax.axis_index("tp")
+    low, high_bit = t % 2, t // 2
+    p = t + 1 - 2 * low
+    q = t + 2 - 4 * high_bit
+    far = 3 - t
+    other = 1 - g
+    rows, chans = u.shape
+    groups, flat = decay.shape[0], st_real.shape[1]
+    own, depth = residual.shape
+    k_loc, ff = gate_h.shape
+    d_loc = down_h.shape[1]
+    n_tp = acts.shape[0]
+    k_half, f_half = k_loc // 2, ff // 2
+    k_piece, d_half = k_half // PIECES, d_loc // HALVES
+    f_piece = f_half * HALVES // PIECES
+
+    barrier = pltpu.get_barrier_semaphore()
+    pl.semaphore_signal(barrier, inc=1, device_id={"tp": p})
+    pl.semaphore_signal(barrier, inc=1, device_id={"tp": q})
+    pl.semaphore_signal(barrier, inc=1, device_id={"grp": other})
+
+    @pl.loop(1, n_sp)
+    def _(d):
+        pl.semaphore_signal(barrier, inc=1, device_id={"sp": (s + d) % n_sp})
+
+    place = pl.ds(pl.multiple_of(s * k_loc, k_loc), k_loc)
+    pairs_of = (
+        (gate_h, w_gate.at[place, :]),
+        (decay_h, decay),
+        (freq_h, freq),
+        (step_h, log_step),
+        (drive_re_h, drive_re),
+        (drive_im_h, drive_im),
+        (u_h, u),
+        (read_re_h, read_re),
+        (read_im_h, read_im),
+        (skip_h, skip),
+        (up_h, w_up.at[place, :]),
+        (down_h, w_down.at[s]),
+        (value_h, value_w),
+        (glu_h, glu_w),
+        (gate_in_h, gate_in),
+        (mix_h, mix_w),
+        (residual_h, residual),
+        (gain_h, gain),
+    )
+    loads = [
+        pltpu.make_async_copy(a, b, load_sem.at[i]) for i, (a, b) in enumerate(pairs_of)
+    ]
+    for load in loads:
+        load.start()
+    pl.semaphore_wait(barrier, 3 + n_sp - 1)
+
+    bufs = (w_gate, w_up, w_down)
+    behind = (s, n_sp - 1 - s)
+    n_early, n_late = 2 * PIECES, PIECES
+
+    def mine(c, i, origin, half):
+        if c < 2:
+            row = pl.multiple_of(origin * k_loc + half * k_half + i * k_piece, k_piece)
+            return bufs[c].at[pl.ds(row, k_piece), :]
+        per = PIECES // HALVES
+        row = pl.multiple_of(half * f_half + (i % per) * f_piece, f_piece)
+        return bufs[c].at[origin, pl.ds(row, f_piece), pl.ds((i // per) * d_half, d_half)]
+
+    def z_copy(side, c, i, origin):
+        piece = mine(c, i, origin, g)
+        return pltpu.make_async_remote_copy(
+            src_ref=piece,
+            dst_ref=piece,
+            send_sem=z_send.at[side, c],
+            recv_sem=z_recv.at[c, i, origin],
+            device_id={"sp": ahead(side)},
+        )
+
+    def y_copy(c, i, origin, half):
+        piece = mine(c, i, origin, half)
+        return pltpu.make_async_remote_copy(
+            src_ref=piece,
+            dst_ref=piece,
+            send_sem=y_send.at[c // 2],
+            recv_sem=y_recv.at[0] if c < 2 else y_late.at[origin, i // (PIECES // HALVES)],
+            device_id={"grp": other},
+        )
+
+    def more_copy(side, c, i):
+        piece = mine(c, i, s, other)
+        return pltpu.make_async_remote_copy(
+            src_ref=piece,
+            dst_ref=piece,
+            send_sem=z_send.at[side, c],
+            recv_sem=z_more.at[0 if c < 2 else 1 + i // (PIECES // HALVES)],
+            device_id={"sp": ahead(side)},
+        )
+
+    def ahead(side):
+        return (s + 1) % n_sp if side == 0 else (s + n_sp - 1) % n_sp
+
+    def source(side, k):
+        return (s + n_sp - k) % n_sp if side == 0 else (s + k) % n_sp
+
+    def own_sends(side, c, pieces):
+        for i in pieces:
+            z_copy(side, c, i, s).start()
+
+    def end_sends(side):
+        for c in range(3):
+            if c == 2:
+                own_sends(side, 2, range(PIECES))
+            for i in range(PIECES):
+                more_copy(side, c, i).start()
+
+    def own_early(c, pieces):
+        for side in range(2):
+            pl.when(behind[side] < n_sp - 1)(functools.partial(own_sends, side, c, pieces))
+
+    def shared(side, k):
+        return behind[side] > 1 if k == 1 else behind[side] >= k
+
+    def onward(side, k, c, i, last):
+        @pl.when(behind[side] < n_sp - 1)
+        def _():
+            z_copy(side, c, i, source(side, k)).start()
+
+        if last:
+
+            @pl.when(jnp.logical_and(behind[side] == k, k < n_sp - 1))
+            def _():
+                own_sends(side, 2, range(PIECES))
+
+    def pass_on(side, k, c, i, last, hold):
+        origin = source(side, k)
+        z_copy(side, c, i, origin).wait_recv()
+        if not hold:
+            onward(side, k, c, i, last)
+
+        @pl.when(shared(side, k))
+        def _():
+            y_copy(c, i, origin, g).start()
+
+    def advance(*slots, hold=False):
+        for n in slots:
+            for side in range(2):
+                if n < n_early * (n_sp - 1):
+                    k, c, i = n // n_early + 1, n % n_early // PIECES, n % PIECES
+                    last = n % n_early == n_early - 1
+                    work = functools.partial(pass_on, side, k, c, i, last, hold)
+                    pl.when(behind[side] >= k)(work)
+                for b in range(1, n_sp):
+                    m = n - n_early * max(b, 2)
+                    if 0 <= m < n_late * b:
+                        work = functools.partial(
+                            pass_on, side, m // n_late + 1, 2, m % n_late, False, False
+                        )
+                        pl.when(behind[side] == b)(work)
+
+    loads[0].wait()
+    own_early(0, range(PIECES))
+
+    for load in loads[1:4]:
+        load.wait()
+    eye = lax.broadcasted_iota(jnp.int32, (groups, groups), 0) == lax.broadcasted_iota(
+        jnp.int32, (groups, groups), 1
+    )
+    step = jnp.exp(jnp.sum(jnp.where(eye, log_step[...], 0.0), axis=1, keepdims=True))
+    rate, turn = decay[...], freq[...]
+    magnitude = jnp.exp(rate * step)
+    bar_re = magnitude * jnp.cos(turn * step)
+    bar_im = magnitude * jnp.sin(turn * step)
+    modulus = rate * rate + turn * turn
+    ratio_re = ((bar_re - 1.0) * rate + bar_im * turn) / modulus
+    ratio_im = (bar_im * rate - (bar_re - 1.0) * turn) / modulus
+    tiles = max(1, 128 // states)
+    lanes = tiles * states
+    part_of = lax.broadcasted_iota(jnp.int32, (1, lanes), 1) // states
+
+    def spread(target, row, value):
+        doubled = jnp.concatenate([value] * tiles, axis=1)
+        for tile in range(groups // tiles):
+            line = doubled[tile * tiles : tile * tiles + 1, :]
+            for j in range(1, tiles):
+                line = jnp.where(part_of == j, doubled[tile * tiles + j : tile * tiles + j + 1, :], line)
+            target[row : row + 1, tile * lanes : (tile + 1) * lanes] = line
+
+    spread(ratio, 0, ratio_re)
+    spread(ratio, 1, ratio_im)
+    up_re, up_im = bar_re, bar_im
+    for n in range(ROWS8):
+        spread(pow_real, n, up_re)
+        spread(pow_imag, n, up_im)
+        up_re, up_im = up_re * bar_re - up_im * bar_im, up_re * bar_im + up_im * bar_re
+
+    for load in loads[4:9]:
+        load.wait()
+    row_group = lax.broadcasted_iota(jnp.int32, (chans, lanes), 0) // width
+    lane = lax.broadcasted_iota(jnp.int32, (chans, lanes), 1)
+    for i, ref in enumerate((drive_re, drive_im, read_re, read_im)):
+        value = jnp.concatenate([ref[...]] * tiles, axis=1)
+        for tile in range(flat // lanes):
+            kept = jnp.where(row_group == (lane + tile * lanes) // states, value, 0.0)
+            at = slice(tile * lanes, (tile + 1) * lanes)
+            for j, piece in enumerate(split(kept)):
+                wide[2 * i + j, :, at] = piece
+
+    @pl.loop(0, rows // own)
+    def _(b):
+        at = pl.ds(pl.multiple_of(b * own, own), own)
+        x = u[at, :]
+        push_re = mm(x, wide[0]) + mm(x, wide[1])
+        push_im = mm(x, wide[2]) + mm(x, wide[3])
+        st_real[at, :] = ratio[0:1, :] * push_re - ratio[1:2, :] * push_im
+        st_imag[at, :] = ratio[0:1, :] * push_im + ratio[1:2, :] * push_re
+
+    sub = lax.broadcasted_iota(jnp.int32, (ROWS8, flat), 0)
+    for i, reach in enumerate((1, 2, 4)):
+        masked[2 * i] = jnp.where(sub >= reach, pow_real[reach - 1 : reach, :], 0.0)
+        masked[2 * i + 1] = jnp.where(sub >= reach, pow_imag[reach - 1 : reach, :], 0.0)
+
+    def scan_step(b, carry):
+        c_re, c_im = carry
+        at = pl.ds(pl.multiple_of(b * ROWS8, ROWS8), ROWS8)
+        x_re, x_im = st_real[at, :], st_imag[at, :]
+        for i, reach in enumerate((1, 2, 4)):
+            m_re, m_im = pltpu.roll(x_re, reach, 0), pltpu.roll(x_im, reach, 0)
+            a_re, a_im = masked[2 * i], masked[2 * i + 1]
+            x_re, x_im = x_re + a_re * m_re - a_im * m_im, x_im + a_re * m_im + a_im * m_re
+        p_re, p_im = pow_real[...], pow_imag[...]
+        x_re, x_im = x_re + p_re * c_re - p_im * c_im, x_im + p_re * c_im + p_im * c_re
+        st_real[at, :] = x_re
+        st_imag[at, :] = x_im
+        return x_re[ROWS8 - 1 :, :], x_im[ROWS8 - 1 :, :]
+
+    zero = jnp.zeros((1, flat), F32)
+    blocks = rows // ROWS8
+    tip = lax.fori_loop(0, blocks // 2, scan_step, (zero, zero))
+    advance(0, hold=True)
+    end_re, end_im = lax.fori_loop(blocks // 2, blocks, scan_step, tip)
+    ends[s, :, :flat] = end_re
+    ends[s, :, flat:] = end_im
+
+    def end_copy(target, origin):
+        return pltpu.make_async_remote_copy(
+            src_ref=ends.at[origin],
+            dst_ref=ends.at[origin],
+            send_sem=end_send.at[target],
+            recv_sem=end_recv.at[origin],
+            device_id={"sp": target},
+        )
+
+    @pl.loop(s + 1, n_sp)
+    def _(later):
+        end_copy(later, s).start()
+
+    for load in loads[10:12]:
+        load.wait()
+    own_early(1, range(PIECES))
+    for side in range(2):
+        pl.when(behind[side] == 0)(functools.partial(end_sends, side))
+        pl.when(behind[side] >= 1)(functools.partial(onward, side, 1, 0, 0, False))
+    advance(1)
+    last_re, last_im = pow_real[ROWS8 - 1 :, :], pow_imag[ROWS8 - 1 :, :]
+    long_re, long_im = last_re, last_im
+    reach = ROWS8
+    while reach < rows:
+        long_re, long_im = long_re * long_re - long_im * long_im, 2.0 * long_re * long_im
+        reach *= 2
+
+    advance(2, 3, 4)
+
+    @pl.loop(0, s)
+    def _(earlier):
+        end_copy((s + 1) % n_sp, earlier).wait_recv()
+
+    def carry_step(j, carry):
+        c_re, c_im = carry
+        e_re, e_im = ends[j, :, :flat], ends[j, :, flat:]
+        n_re = long_re * c_re - long_im * c_im + e_re
+        n_im = long_re * c_im + long_im * c_re + e_im
+        return jnp.where(j < s, n_re, c_re), jnp.where(j < s, n_im, c_im)
+
+    carry = lax.fori_loop(0, n_sp - 1, carry_step, (zero, zero))
+
+    def lift(b, carry):
+        c_re, c_im = carry
+        at = pl.ds(pl.multiple_of(b * ROWS8, ROWS8), ROWS8)
+        p_re, p_im = pow_real[...], pow_imag[...]
+        st_real[at, :] = st_real[at, :] + p_re * c_re - p_im * c_im
+        st_imag[at, :] = st_imag[at, :] + p_re * c_im + p_im * c_re
+        return last_re * c_re - last_im * c_im, last_re * c_im + last_im * c_re
+
+    carry = lax.fori_loop(0, blocks // 2, lift, carry)
+    advance(5)
+    lax.fori_loop(blocks // 2, blocks, lift, carry)
+    loads[9].wait()
+
+    def read_block(b):
+        at = pl.ds(pl.multiple_of(b * own, own), own)
+        high, small = split(st_real[at, :])
+        y = mm_t(high, wide[4]) + mm_t(small, wide[4]) + mm_t(high, wide[5])
+        high, small = split(st_imag[at, :])
+        y = y - (mm_t(high, wide[6]) + mm_t(small, wide[6]) + mm_t(high, wide[7]))
+        y = y + skip[...] * u[at, :].astype(F32)
+        acts[t, at, :] = jax.nn.gelu(y).astype(BF)
+
+    half_rows = rows // own // 2
+    pl.loop(0, half_rows)(read_block)
+    advance(6)
+    pl.loop(half_rows, rows // own)(read_block)
+    advance(7)
+
+    def gather_tp(buf, lane_no, between, later):
+        def copy(slot, kind, target):
+            return pltpu.make_async_remote_copy(
+                src_ref=buf.at[slot],
+                dst_ref=buf.at[slot],
+                send_sem=ag_send.at[lane_no, kind],
+                recv_sem=ag_recv.at[lane_no, kind],
+                device_id={"tp": target},
+            )
+
+        sent = [copy(t, 0, q), copy(t, 1, p)]
+        for item in sent:
+            item.start()
+        between()
+        copy(q, 0, q).wait_recv()
+        relayed = copy(q, 2, p)
+        relayed.start()
+        later()
+        copy(p, 1, p).wait_recv()
+        copy(far, 2, p).wait_recv()
+        return sent + [relayed]
+
+    def rs_pair(index):
+        return pltpu.make_async_remote_copy(
+            src_ref=part.at[(far, p)[index]],
+            dst_ref=rx_pair.at[index],
+            send_sem=rs_send.at[index],
+            recv_sem=rs_recv.at[index],
+            device_id={"tp": p},
+        )
+
+    across = pltpu.make_async_remote_copy(
+        src_ref=relay,
+        dst_ref=rx_far,
+        send_sem=rs_send.at[2],
+        recv_sem=rs_recv.at[2],
+        device_id={"tp": q},
+    )
+
+    pending = gather_tp(acts, 0, lambda: advance(8, 9), lambda: advance(10))
+    for load in loads[12:]:
+        load.wait()
+
+    def mix_block(r):
+        at = pl.ds(pl.multiple_of(r * own, own), own)
+        value = jnp.zeros((own, value_w.shape[1]), F32)
+        gated = value
+        for j in range(n_tp):
+            a = acts[j, at, :]
+            value = value + mm(a, value_w[j * chans : (j + 1) * chans, :])
+            gated = gated + mm(a, glu_w[j * chans : (j + 1) * chans, :])
+        mixed = jax.nn.sigmoid(gate_in[at, :].astype(F32)) * value * jax.nn.sigmoid(gated)
+        part[r] = mm(mixed.astype(BF), mix_w[...]).astype(BF)
+
+    mix_block(far)
+    rs_pair(0).start()
+    advance(11)
+    mix_block(q)
+    rs_pair(0).wait_recv()
+    relay[...] = (part[q].astype(F32) + rx_pair[0].astype(F32)).astype(BF)
+    across.start()
+    advance(12)
+    mix_block(p)
+    rs_pair(1).start()
+    mix_block(t)
+    advance(13, 14, 15, 16, 17)
+    rs_pair(1).wait_recv()
+    across.wait_recv()
+    pending += [rs_pair(0), rs_pair(1), across]
+    near = part[t].astype(F32) + rx_pair[1].astype(F32)
+    x = residual[...].astype(F32) + (near + rx_far[...].astype(F32))
+    inner[...] = x
+    scale = lax.rsqrt(jnp.mean(x * x, axis=-1, keepdims=True) + EPSILON)
+    normed[t] = (x * scale * gain[...]).astype(BF)
+
+    pending += gather_tp(normed, 1, lambda: advance(18, 19, 20, 21, 22, 23), lambda: None)
+
+    advance(24)
+
+    def await_bytes(sem, ref):
+        pltpu.make_async_copy(ref, ref, sem).wait()
+
+    advance(25)
+    near_end = jnp.logical_or(behind[0] == 1, behind[1] == 1)
+
+    @pl.when(near_end)
+    def _():
+        await_bytes(z_more.at[0], w_gate.at[:k_loc, :])
+        await_bytes(y_recv.at[0], w_gate.at[: (n_sp - 2) * k_loc, :])
+
+    @pl.when(jnp.logical_not(near_end))
+    def _():
+        await_bytes(y_recv.at[0], w_gate.at[: (n_sp - 1) * k_loc, :])
+
+    advance(26)
+
+    def hidden_block(r):
+        x = normed[r]
+        hidden[r] = (jax.nn.silu(mm(x, w_gate[...])) * mm(x, w_up[...])).astype(BF)
+
+    pl.loop(0, n_tp // 2)(hidden_block)
+    advance(27)
+    pl.loop(n_tp // 2, n_tp)(hidden_block)
+    advance(28)
+
+    def col_pair(o, h, index):
+        return pltpu.make_async_remote_copy(
+            src_ref=c_part.at[o, h, (far, p)[index]],
+            dst_ref=c_in.at[o, h, index],
+            send_sem=c_send.at[0],
+            recv_sem=c_recv.at[o, h if index == 0 else HALVES],
+            device_id={"tp": p},
+        )
+
+    def col_far(o, h):
+        return pltpu.make_async_remote_copy(
+            src_ref=c_relay.at[o, h],
+            dst_ref=c_in.at[o, h, 2],
+            send_sem=c_send.at[0],
+            recv_sem=c_recv.at[o, HALVES],
+            device_id={"tp": q},
+        )
+
+    def column(o, h):
+        weight = w_down.at[o, :, h * d_half : (h + 1) * d_half]
+        for r, index in ((far, 0), (p, 1), (q, None), (t, None)):
+            c_part[o, h, r] = mm(hidden[r], weight[...]).astype(BF)
+            if index is not None:
+                col_pair(o, h, index).start()
+        col_pair(o, h, 0).wait_recv()
+        both = c_part[o, h, q].astype(F32) + c_in[o, h, 0].astype(F32)
+        c_relay[o, h] = both.astype(BF)
+        col_far(o, h).start()
+
+    def settle(o):
+        await_bytes(c_recv.at[o, HALVES], c_in.at[o, :, 1:3])
+        for h in range(HALVES):
+            near = c_part[o, h, t].astype(F32) + c_in[o, h, 1].astype(F32)
+            at = pl.ds(pl.multiple_of(o * d_loc + h * d_half, d_half), d_half)
+            out[:, at] = (inner[:, at] + 0.5 * (near + c_in[o, h, 2].astype(F32))).astype(BF)
+
+    def both_sides(k, work):
+        for side in range(2):
+            pl.when(behind[side] >= k)(functools.partial(work, side, k))
+
+    def next_column(h, side, k):
+        origin = source(side, k)
+        row = pl.multiple_of(other * f_half, f_half)
+        came = w_down.at[origin, pl.ds(row, f_half), h * d_half : (h + 1) * d_half]
+
+        @pl.when(shared(side, k))
+        def _():
+            await_bytes(y_late.at[origin, h], came)
+
+        if k == 1:
+
+            @pl.when(behind[side] == 1)
+            def _():
+                await_bytes(z_more.at[1 + h], came)
+
+        column(origin, h)
+
+    def next_settle(side, k):
+        settle(source(side, k))
+
+    column(s, 0)
+    column(s, 1)
+    advance(29)
+    both_sides(1, functools.partial(next_column, 0))
+    advance(30)
+    both_sides(1, functools.partial(next_column, 1))
+    advance(31)
+    settle(s)
+    advance(32)
+    both_sides(2, functools.partial(next_column, 0))
+    advance(33, 34)
+    both_sides(2, functools.partial(next_column, 1))
+    advance(35)
+    both_sides(1, next_settle)
+    both_sides(3, functools.partial(next_column, 0))
+    both_sides(2, next_settle)
+    for item in pending:
+        item.wait_send()
+
+    @pl.loop(s + 1, n_sp)
+    def _(later):
+        end_copy(later, s).wait_send()
+
+    def sent(side, b):
+        count = max(2, b + 1)
+        for c in range(2):
+            await_bytes(z_send.at[side, c], w_gate.at[: count * k_half, :])
+        await_bytes(z_send.at[side, 2], w_down.at[:count, :f_half, :])
+
+    for side in range(2):
+        for b in range(n_sp - 1):
+            pl.when(behind[side] == b)(functools.partial(sent, side, b))
+
+    def exchanged(count):
+        await_bytes(y_send.at[0], w_gate.at[: count * k_loc, :])
+        await_bytes(y_send.at[1], w_down.at[:count, :f_half, :])
+
+    pl.when(near_end)(functools.partial(exchanged, n_sp - 2))
+    pl.when(jnp.logical_not(near_end))(functools.partial(exchanged, n_sp - 1))
+    both_sides(3, functools.partial(next_column, 1))
+    both_sides(3, next_settle)
+    await_bytes(c_send.at[0], c_in)
+
+
+def quick(
+    residual,
+    state_input,
+    gate_input,
+    decay_real,
+    frequency,
+    log_step,
+    drive_real,
+    drive_imag,
+    read_real,
+    read_imag,
+    skip_gain,
+    value_weight,
+    glu_weight,
+    mix_weight,
+    norm_gain,
+    mlp_gate,
+    mlp_up,
+    mlp_down,
+):
+    n_sp, n_tp = lax.axis_size("sp"), lax.axis_size("tp")
+    groups, states, width = drive_real.shape
+    flat, chans = groups * states, groups * width
+    rows = state_input.shape[0]
+    own, depth = residual.shape
+    k_loc, ff = mlp_gate.shape
+    d_loc = mlp_down.shape[1]
+    d_half = d_loc // HALVES
+    hbm = pl.BlockSpec(memory_space=pltpu.HBM)
+    dma = pltpu.SemaphoreType.DMA
+    operands = (
+        residual,
+        state_input,
+        gate_input,
+        decay_real,
+        frequency,
+        log_step[None, :],
+        drive_real.transpose(0, 2, 1).reshape(chans, states),
+        drive_imag.transpose(0, 2, 1).reshape(chans, states),
+        read_real.reshape(chans, states),
+        read_imag.reshape(chans, states),
+        skip_gain[None, :],
+        value_weight,
+        glu_weight,
+        mix_weight,
+        norm_gain[None, :],
+        mlp_gate,
+        mlp_up,
+        mlp_down,
+    )
+    return pl.pallas_call(
+        functools.partial(quick_kernel, n_sp, width, states),
+        out_shape=pltpu.VMEM((own, depth), BF),
+        in_specs=[hbm] * len(operands),
+        out_specs=pl.BlockSpec(memory_space=pltpu.VMEM),
+        scratch_shapes=[pltpu.VMEM(x.shape, x.dtype) for x in operands[:15]]
+        + [
+            pltpu.VMEM((n_sp * k_loc, ff), BF),
+            pltpu.VMEM((n_sp * k_loc, ff), BF),
+            pltpu.VMEM((n_sp, ff, d_loc), BF),
+            pltpu.VMEM((8, chans, flat), BF),
+            pltpu.VMEM((ROWS8, flat), F32),
+            pltpu.VMEM((ROWS8, flat), F32),
+            pltpu.VMEM((2, flat), F32),
+            pltpu.VMEM((rows, flat), F32),
+            pltpu.VMEM((rows, flat), F32),
+            pltpu.VMEM((6, ROWS8, flat), F32),
+            pltpu.VMEM((n_sp, 1, 2 * flat), F32),
+            pltpu.VMEM((n_tp, rows, chans), BF),
+            pltpu.VMEM((n_tp, own, depth), BF),
+            pltpu.VMEM((2, own, depth), BF),
+            pltpu.VMEM((own, depth), BF),
+            pltpu.VMEM((own, depth), BF),
+            pltpu.VMEM((own, depth), F32),
+            pltpu.VMEM((n_tp, own, depth), BF),
+            pltpu.VMEM((n_tp, own, ff), BF),
+            pltpu.VMEM((n_sp, HALVES, n_tp, own, d_half), BF),
+            pltpu.VMEM((n_sp, HALVES, 3, own, d_half), BF),
+            pltpu.VMEM((n_sp, HALVES, own, d_half), BF),
+            dma((len(operands),)),
+            dma((n_sp,)),
+            dma((n_sp,)),
+            dma((2, 3)),
+            dma((3, PIECES, n_sp)),
+            dma((2,)),
+            dma((1,)),
+            dma((n_sp, HALVES)),
+            dma((1 + HALVES,)),
+            dma((2, 3)),
+            dma((2, 3)),
+            dma((3,)),
+            dma((3,)),
+            dma((1,)),
+            dma((n_sp, HALVES + 1)),
+        ],
+        compiler_params=pltpu.CompilerParams(
+            collective_id=0, has_side_effects=True, vmem_limit_bytes=60 * 1024 * 1024
+        ),
+    )(*operands)
+
+
 def solution(mesh):
     placed = (
         P(("grp", "sp", "tp"), None),
@@ -780,7 +1478,9 @@
         P("sp", "tp"),
         P("tp", "sp"),
     )
-    body = fused if (mesh.shape["tp"], mesh.shape["grp"]) == (4, 2) else shards
+    body = shards
+    if (mesh.shape["tp"], mesh.shape["grp"]) == (4, 2):
+        body = quick if mesh.shape["sp"] == 4 else fused
     return jax.shard_map(
         body, mesh=mesh, in_specs=placed, out_specs=P(("grp", "sp", "tp"), None), check_vma=False
     )

time: 136 us -> 95.5 us (0.70)
  Pallas kernels: 128 us -> 94.6 us
  other arithmetic: 5.44 us -> 0 us
  local copies, waits for them, and re-layouts: 2.68 us -> 0.8 us
    pallas_call x1, Pallas kernels: 128 us -> 94.6 us  [quick(): pl.pallas_call(functools.partial(quick_kernel, n_sp, width, states), out_...]
    concatenate x2 -> x0, other arithmetic: 2.76 us -> none  [tiled(): return jnp.concatenate([x.reshape(chans, states)] * times, axis=1)]
where the time goes in v2:
time: 95.5 us; the launch traced here: 95.4 us
  Pallas kernels  94.6 us (99%)
    pallas_call x1, Pallas kernels, quick(): pl.pallas_call(functools.partial(quick_kernel, n_sp, width, states), out_...  94.6 us

profile of v2, /device:TPU:0, one launch (start us, length us, event | category | flops | bytes accessed | tf_op | source)
XLA Modules:
  0.0 95.4 jit_solution(4712178729619952390)
XLA Ops:
  0.0 94.6 %shard_map.172 = bf16[128,2048]{1,0:T(8,128)(2,1)S(1)} custom-call(bf16[128,2048]{1,0:T(8,128)(2,1)} %residual_h.1, bf16[512,256]{1,0:T(8,128)(2,1)} %u_h.1, bf16[512,512]{1,0:T(8,128)(2,1)} %gate_in_h.1, f32[16,64]{1,0:T(8,128)} %decay_h.1, f32[16,64]{1,0:T(8,128)} %freq_h.1, f32[1,16]{1,0:T(1,128)} %bitcast.17, f32[256,64]{1,0:T(8,128)} %bitcast.11, ...), custom_call_target="tpu_custom_call" | custom-call | tf_op jit(solution)/shard_map/pallas_call | solution.py:1409
  94.6 0.8 copy.20

commit v3 on v2

--- a/solution.py
+++ b/solution.py
@@ -11,6 +11,7 @@
 ROWS8 = 8
 PIECES = 4
 HALVES = 2
+PER = PIECES // HALVES
 
 HIGH = lax.Precision.HIGHEST
 EPSILON = 1e-06
@@ -830,6 +831,7 @@
     y_recv,
     y_late,
     z_more,
+    z_last,
     ag_send,
     ag_recv,
     rs_send,
@@ -894,13 +896,15 @@
     behind = (s, n_sp - 1 - s)
     n_early, n_late = 2 * PIECES, PIECES
 
+    def await_bytes(sem, ref):
+        pltpu.make_async_copy(ref, ref, sem).wait()
+
     def mine(c, i, origin, half):
         if c < 2:
             row = pl.multiple_of(origin * k_loc + half * k_half + i * k_piece, k_piece)
             return bufs[c].at[pl.ds(row, k_piece), :]
-        per = PIECES // HALVES
-        row = pl.multiple_of(half * f_half + (i % per) * f_piece, f_piece)
-        return bufs[c].at[origin, pl.ds(row, f_piece), pl.ds((i // per) * d_half, d_half)]
+        row = pl.multiple_of(half * f_half + (i % PER) * f_piece, f_piece)
+        return bufs[c].at[origin, pl.ds(row, f_piece), pl.ds((i // PER) * d_half, d_half)]
 
     def z_copy(side, c, i, origin):
         piece = mine(c, i, origin, g)
@@ -908,7 +912,7 @@
             src_ref=piece,
             dst_ref=piece,
             send_sem=z_send.at[side, c],
-            recv_sem=z_recv.at[c, i, origin],
+            recv_sem=z_recv.at[c, i, origin - side],
             device_id={"sp": ahead(side)},
         )
 
@@ -918,7 +922,7 @@
             src_ref=piece,
             dst_ref=piece,
             send_sem=y_send.at[c // 2],
-            recv_sem=y_recv.at[0] if c < 2 else y_late.at[origin, i // (PIECES // HALVES)],
+            recv_sem=y_recv.at[0] if c < 2 else y_late.at[origin, i // (PER)],
             device_id={"grp": other},
         )
 
@@ -928,9 +932,31 @@
             src_ref=piece,
             dst_ref=piece,
             send_sem=z_send.at[side, c],
-            recv_sem=z_more.at[0 if c < 2 else 1 + i // (PIECES // HALVES)],
+            recv_sem=z_more.at[0 if c < 2 else 1 + HALVES * (i == PIECES - 1) + i // PER],
             device_id={"sp": ahead(side)},
         )
+
+    def last_copy(side, k):
+        piece = mine(2, PIECES - 1, source(side, k), other)
+        return pltpu.make_async_remote_copy(
+            src_ref=piece,
+            dst_ref=piece,
+            send_sem=z_send.at[side, 2],
+            recv_sem=z_last.at[0],
+            device_id={"sp": ahead(side)},
+        )
+
+    def last_on(side, b):
+        if b == 1:
+            await_bytes(z_more.at[1 + HALVES + (PIECES - 1) // PER], mine(2, 0, s, g))
+        else:
+            last_copy(side, b).wait_recv()
+        if b < n_sp - 1:
+            last_copy(side, b).start()
+
+    def last_advance(b):
+        for side in range(2):
+            pl.when(behind[side] == b)(functools.partial(last_on, side, b))
 
     def ahead(side):
         return (s + 1) % n_sp if side == 0 else (s + n_sp - 1) % n_sp
@@ -973,7 +999,9 @@
         if not hold:
             onward(side, k, c, i, last)
 
-        @pl.when(shared(side, k))
+        only_z = c == 2 and i == PIECES - 1
+
+        @pl.when(behind[side] > k if only_z else shared(side, k))
         def _():
             y_copy(c, i, origin, g).start()
 
@@ -1225,9 +1253,7 @@
     pending += gather_tp(normed, 1, lambda: advance(18, 19, 20, 21, 22, 23), lambda: None)
 
     advance(24)
-
-    def await_bytes(sem, ref):
-        pltpu.make_async_copy(ref, ref, sem).wait()
+    last_advance(1)
 
     advance(25)
     near_end = jnp.logical_or(behind[0] == 1, behind[1] == 1)
@@ -1251,6 +1277,7 @@
     advance(27)
     pl.loop(n_tp // 2, n_tp)(hidden_block)
     advance(28)
+    last_advance(2)
 
     def col_pair(o, h, index):
         return pltpu.make_async_remote_copy(
@@ -1296,16 +1323,24 @@
         origin = source(side, k)
         row = pl.multiple_of(other * f_half, f_half)
         came = w_down.at[origin, pl.ds(row, f_half), h * d_half : (h + 1) * d_half]
-
-        @pl.when(shared(side, k))
+        piece = mine(2, h * PER, origin, other)
+        pairs = h == HALVES - 1
+
+        @pl.when(behind[side] > k if pairs else shared(side, k))
         def _():
             await_bytes(y_late.at[origin, h], came)
 
+        if pairs and k > 1:
+
+            @pl.when(behind[side] == k)
+            def _():
+                await_bytes(y_late.at[origin, h], piece)
+
         if k == 1:
 
             @pl.when(behind[side] == 1)
             def _():
-                await_bytes(z_more.at[1 + h], came)
+                await_bytes(z_more.at[1 + h], piece if pairs else came)
 
         column(origin, h)
 
@@ -1339,7 +1374,8 @@
         count = max(2, b + 1)
         for c in range(2):
             await_bytes(z_send.at[side, c], w_gate.at[: count * k_half, :])
-        await_bytes(z_send.at[side, 2], w_down.at[:count, :f_half, :])
+        count = count * PIECES + (b > 0)
+        await_bytes(z_send.at[side, 2], w_gate.at[: count * k_piece, :])
 
     for side in range(2):
         for b in range(n_sp - 1):
@@ -1347,10 +1383,11 @@
 
     def exchanged(count):
         await_bytes(y_send.at[0], w_gate.at[: count * k_loc, :])
-        await_bytes(y_send.at[1], w_down.at[:count, :f_half, :])
+        await_bytes(y_send.at[1], w_gate.at[: (count * PIECES - 1) * k_piece, :])
 
     pl.when(near_end)(functools.partial(exchanged, n_sp - 2))
     pl.when(jnp.logical_not(near_end))(functools.partial(exchanged, n_sp - 1))
+    last_advance(3)
     both_sides(3, functools.partial(next_column, 1))
     both_sides(3, next_settle)
     await_bytes(c_send.at[0], c_in)
@@ -1439,11 +1476,12 @@
             dma((n_sp,)),
             dma((n_sp,)),
             dma((2, 3)),
-            dma((3, PIECES, n_sp)),
+            dma((3, PIECES, n_sp - 1)),
             dma((2,)),
             dma((1,)),
             dma((n_sp, HALVES)),
-            dma((1 + HALVES,)),
+            dma((1 + 2 * HALVES,)),
+            dma((1,)),
             dma((2, 3)),
             dma((2, 3)),
             dma((3,)),

time: 95.5 us -> 93.4 us (0.978)
  Pallas kernels: 94.6 us -> 92.4 us
    pallas_call x1, Pallas kernels: 94.6 us -> 92.4 us  [quick(): pl.pallas_call(functools.partial(quick_kernel, n_sp, width, states), out_...]
where the time goes in v3:
time: 93.4 us; the launch traced here: 93.3 us
  Pallas kernels  92.4 us (99%)
    pallas_call x1, Pallas kernels, quick(): pl.pallas_call(functools.partial(quick_kernel, n_sp, width, states), out_...  92.4 us

profile of v3, /device:TPU:0, one launch (start us, length us, event | category | flops | bytes accessed | tf_op | source)
XLA Modules:
  0.0 93.3 jit_solution(4677381495556002078)
XLA Ops:
  0.0 92.4 %shard_map.172 = bf16[128,2048]{1,0:T(8,128)(2,1)S(1)} custom-call(bf16[128,2048]{1,0:T(8,128)(2,1)} %residual_h.1, bf16[512,256]{1,0:T(8,128)(2,1)} %u_h.1, bf16[512,512]{1,0:T(8,128)(2,1)} %gate_in_h.1, f32[16,64]{1,0:T(8,128)} %decay_h.1, f32[16,64]{1,0:T(8,128)} %freq_h.1, f32[1,16]{1,0:T(1,128)} %bitcast.17, f32[256,64]{1,0:T(8,128)} %bitcast.11, ...), custom_call_target="tpu_custom_call" | custom-call | tf_op jit(solution)/shard_map/pallas_call | solution.py:1446
  92.5 0.8 copy.20

commit v4 on v2

--- a/solution.py
+++ b/solution.py
@@ -11,6 +11,7 @@
 ROWS8 = 8
 PIECES = 4
 HALVES = 2
+PER = PIECES // HALVES
 
 HIGH = lax.Precision.HIGHEST
 EPSILON = 1e-06
@@ -821,6 +822,10 @@
     c_part,
     c_in,
     c_relay,
+    guest,
+    g_hidden,
+    g_out,
+    g_in,
     load_sem,
     end_send,
     end_recv,
@@ -830,6 +835,10 @@
     y_recv,
     y_late,
     z_more,
+    g_send,
+    g_recv,
+    b_send,
+    b_recv,
     ag_send,
     ag_recv,
     rs_send,
@@ -894,13 +903,15 @@
     behind = (s, n_sp - 1 - s)
     n_early, n_late = 2 * PIECES, PIECES
 
+    def await_bytes(sem, ref):
+        pltpu.make_async_copy(ref, ref, sem).wait()
+
     def mine(c, i, origin, half):
         if c < 2:
             row = pl.multiple_of(origin * k_loc + half * k_half + i * k_piece, k_piece)
             return bufs[c].at[pl.ds(row, k_piece), :]
-        per = PIECES // HALVES
-        row = pl.multiple_of(half * f_half + (i % per) * f_piece, f_piece)
-        return bufs[c].at[origin, pl.ds(row, f_piece), pl.ds((i // per) * d_half, d_half)]
+        row = pl.multiple_of(half * f_half + (i % PER) * f_piece, f_piece)
+        return bufs[c].at[origin, pl.ds(row, f_piece), pl.ds((i // PER) * d_half, d_half)]
 
     def z_copy(side, c, i, origin):
         piece = mine(c, i, origin, g)
@@ -908,7 +919,7 @@
             src_ref=piece,
             dst_ref=piece,
             send_sem=z_send.at[side, c],
-            recv_sem=z_recv.at[c, i, origin],
+            recv_sem=z_recv.at[c, i, origin - side],
             device_id={"sp": ahead(side)},
         )
 
@@ -918,7 +929,7 @@
             src_ref=piece,
             dst_ref=piece,
             send_sem=y_send.at[c // 2],
-            recv_sem=y_recv.at[0] if c < 2 else y_late.at[origin, i // (PIECES // HALVES)],
+            recv_sem=y_recv.at[0] if c < 2 else y_late.at[origin, i // (PER)],
             device_id={"grp": other},
         )
 
@@ -928,7 +939,7 @@
             src_ref=piece,
             dst_ref=piece,
             send_sem=z_send.at[side, c],
-            recv_sem=z_more.at[0 if c < 2 else 1 + i // (PIECES // HALVES)],
+            recv_sem=z_more.at[0 if c < 2 else 1 + i // PER],
             device_id={"sp": ahead(side)},
         )
 
@@ -946,8 +957,53 @@
         for c in range(3):
             if c == 2:
                 own_sends(side, 2, range(PIECES))
-            for i in range(PIECES):
-                more_copy(side, c, i).start()
+            else:
+                for i in range(PIECES):
+                    more_copy(side, c, i).start()
+
+    inner_one = jnp.logical_or(behind[0] == 1, behind[1] == 1)
+    end_one = jnp.logical_not(inner_one)
+    mate = s + 1 - 2 * (s % 2)
+    taken = (1 - s // (n_sp // 2)) * (n_sp - 1)
+    e_rows = own // 2
+
+    def guest_copy(h):
+        rows_of = pl.ds(h * e_rows, e_rows)
+        return pltpu.make_async_remote_copy(
+            src_ref=normed.at[t, rows_of, :],
+            dst_ref=guest.at[t, rows_of, :],
+            send_sem=g_send.at[0],
+            recv_sem=g_recv.at[0, h],
+            device_id={"sp": mate},
+        )
+
+    def guest_tp(h, slot, kind, target):
+        piece = guest.at[slot, pl.ds(h * e_rows, e_rows), :]
+        return pltpu.make_async_remote_copy(
+            src_ref=piece,
+            dst_ref=piece,
+            send_sem=g_send.at[(2, 0, 1)[kind]],
+            recv_sem=g_recv.at[1 + kind, h],
+            device_id={"tp": target},
+        )
+
+    guest_cross = pltpu.make_async_remote_copy(
+        src_ref=normed.at[q, pl.ds(e_rows, e_rows), :],
+        dst_ref=guest.at[q, pl.ds(e_rows, e_rows), :],
+        send_sem=g_send.at[2],
+        recv_sem=g_recv.at[1, 1],
+        device_id={"sp": mate},
+    )
+
+    def guest_take(h):
+        guest_copy(h).wait_recv()
+        if h == 0:
+            guest_tp(h, t, 0, q).start()
+        guest_tp(h, t, 1, p).start()
+
+    def guest_relay(h):
+        guest_tp(h, q, 0, q).wait_recv()
+        guest_tp(h, q, 2, p).start()
 
     def own_early(c, pieces):
         for side in range(2):
@@ -987,10 +1043,10 @@
                     pl.when(behind[side] >= k)(work)
                 for b in range(1, n_sp):
                     m = n - n_early * max(b, 2)
-                    if 0 <= m < n_late * b:
-                        work = functools.partial(
-                            pass_on, side, m // n_late + 1, 2, m % n_late, False, False
-                        )
+                    k = m // n_late + 1
+                    if 0 <= m and k <= min(b, n_sp - 2):
+                        stop = k == b == n_sp - 2
+                        work = functools.partial(pass_on, side, k, 2, m % n_late, False, stop)
                         pl.when(behind[side] == b)(work)
 
     loads[0].wait()
@@ -1160,12 +1216,12 @@
         sent = [copy(t, 0, q), copy(t, 1, p)]
         for item in sent:
             item.start()
+        copy(p, 1, p).wait_recv()
         between()
         copy(q, 0, q).wait_recv()
         relayed = copy(q, 2, p)
         relayed.start()
         later()
-        copy(p, 1, p).wait_recv()
         copy(far, 2, p).wait_recv()
         return sent + [relayed]
 
@@ -1190,28 +1246,29 @@
     for load in loads[12:]:
         load.wait()
 
-    def mix_block(r):
-        at = pl.ds(pl.multiple_of(r * own, own), own)
-        value = jnp.zeros((own, value_w.shape[1]), F32)
+    near_half = high_bit
+    duo = n_tp // 2
+
+    def mix_half(b):
+        at = pl.ds(pl.multiple_of(b * duo * own, own), duo * own)
+        value = jnp.zeros((duo * own, value_w.shape[1]), F32)
         gated = value
         for j in range(n_tp):
             a = acts[j, at, :]
             value = value + mm(a, value_w[j * chans : (j + 1) * chans, :])
             gated = gated + mm(a, glu_w[j * chans : (j + 1) * chans, :])
         mixed = jax.nn.sigmoid(gate_in[at, :].astype(F32)) * value * jax.nn.sigmoid(gated)
-        part[r] = mm(mixed.astype(BF), mix_w[...]).astype(BF)
-
-    mix_block(far)
+        product = mm(mixed.astype(BF), mix_w[...]).astype(BF)
+        part[pl.ds(b * duo, duo)] = product.reshape(duo, own, depth)
+
+    mix_half(1 - near_half)
     rs_pair(0).start()
-    advance(11)
-    mix_block(q)
+    advance(11, 12)
     rs_pair(0).wait_recv()
     relay[...] = (part[q].astype(F32) + rx_pair[0].astype(F32)).astype(BF)
     across.start()
-    advance(12)
-    mix_block(p)
+    mix_half(near_half)
     rs_pair(1).start()
-    mix_block(t)
     advance(13, 14, 15, 16, 17)
     rs_pair(1).wait_recv()
     across.wait_recv()
@@ -1222,34 +1279,58 @@
     scale = lax.rsqrt(jnp.mean(x * x, axis=-1, keepdims=True) + EPSILON)
     normed[t] = (x * scale * gain[...]).astype(BF)
 
-    pending += gather_tp(normed, 1, lambda: advance(18, 19, 20, 21, 22, 23), lambda: None)
-
-    advance(24)
-
-    def await_bytes(sem, ref):
-        pltpu.make_async_copy(ref, ref, sem).wait()
-
-    advance(25)
-    near_end = jnp.logical_or(behind[0] == 1, behind[1] == 1)
-
-    @pl.when(near_end)
+
+    @pl.when(end_one)
     def _():
+        for h in range(2):
+            guest_copy(h).start()
+
+    def gated_half(rows_in, rows_out, b):
+        x = rows_in[pl.ds(b * duo, duo)].reshape(duo * own, depth)
+        both = (jax.nn.silu(mm(x, w_gate[...])) * mm(x, w_up[...])).astype(BF)
+        rows_out[pl.ds(b * duo, duo)] = both.reshape(duo, own, ff)
+
+    def inner_first():
         await_bytes(z_more.at[0], w_gate.at[:k_loc, :])
         await_bytes(y_recv.at[0], w_gate.at[: (n_sp - 2) * k_loc, :])
-
-    @pl.when(jnp.logical_not(near_end))
+        gated_half(normed, hidden, near_half)
+
+    def while_gathering():
+        advance(18, 19)
+        pl.when(inner_one)(inner_first)
+        advance(20, 21, 22)
+        pl.when(inner_one)(lambda: guest_take(0))
+        advance(23)
+
+    pending += gather_tp(normed, 1, while_gathering, lambda: None)
+
+    advance(24)
+
+    @pl.when(end_one)
+    def _():
+        guest_cross.start()
+        for side in range(2):
+
+            @pl.when(behind[side] == 0)
+            def _():
+                for i in range(PIECES):
+                    more_copy(side, 2, i).start()
+
+    @pl.when(inner_one)
+    def _():
+        guest_take(1)
+        gated_half(normed, hidden, 1 - near_half)
+
+    advance(25)
+
+    @pl.when(end_one)
     def _():
         await_bytes(y_recv.at[0], w_gate.at[: (n_sp - 1) * k_loc, :])
 
     advance(26)
-
-    def hidden_block(r):
-        x = normed[r]
-        hidden[r] = (jax.nn.silu(mm(x, w_gate[...])) * mm(x, w_up[...])).astype(BF)
-
-    pl.loop(0, n_tp // 2)(hidden_block)
+    pl.when(end_one)(lambda: gated_half(normed, hidden, near_half))
     advance(27)
-    pl.loop(n_tp // 2, n_tp)(hidden_block)
+    pl.when(end_one)(lambda: gated_half(normed, hidden, 1 - near_half))
     advance(28)
 
     def col_pair(o, h, index):
@@ -1270,29 +1351,47 @@
             device_id={"tp": q},
         )
 
-    def column(o, h):
+    def column(o, h, rows_in=hidden, slot=None):
+        slot = o if slot is None else slot
         weight = w_down.at[o, :, h * d_half : (h + 1) * d_half]
-        for r, index in ((far, 0), (p, 1), (q, None), (t, None)):
-            c_part[o, h, r] = mm(hidden[r], weight[...]).astype(BF)
-            if index is not None:
-                col_pair(o, h, index).start()
+        product = mm(rows_in[...].reshape(n_tp * own, ff), weight[...]).astype(BF)
+        c_part[slot, h] = product.reshape(n_tp, own, d_half)
+        for index in range(2):
+            col_pair(slot, h, index).start()
+
+    def relay_on(o, h):
         col_pair(o, h, 0).wait_recv()
         both = c_part[o, h, q].astype(F32) + c_in[o, h, 0].astype(F32)
         c_relay[o, h] = both.astype(BF)
         col_far(o, h).start()
 
+    def total(o, h):
+        near = c_part[o, h, t].astype(F32) + c_in[o, h, 1].astype(F32)
+        return near + c_in[o, h, 2].astype(F32)
+
+    def put(o, h, value):
+        at = pl.ds(pl.multiple_of(o * d_loc + h * d_half, d_half), d_half)
+        out[:, at] = (inner[:, at] + 0.5 * value).astype(BF)
+
+    def back_copy(h):
+        return pltpu.make_async_remote_copy(
+            src_ref=g_out.at[h],
+            dst_ref=g_in.at[h],
+            send_sem=b_send.at[0],
+            recv_sem=b_recv.at[h],
+            device_id={"sp": mate},
+        )
+
     def settle(o):
         await_bytes(c_recv.at[o, HALVES], c_in.at[o, :, 1:3])
         for h in range(HALVES):
-            near = c_part[o, h, t].astype(F32) + c_in[o, h, 1].astype(F32)
-            at = pl.ds(pl.multiple_of(o * d_loc + h * d_half, d_half), d_half)
-            out[:, at] = (inner[:, at] + 0.5 * (near + c_in[o, h, 2].astype(F32))).astype(BF)
+            put(o, h, total(o, h))
 
     def both_sides(k, work):
         for side in range(2):
             pl.when(behind[side] >= k)(functools.partial(work, side, k))
 
-    def next_column(h, side, k):
+    def land(h, side, k):
         origin = source(side, k)
         row = pl.multiple_of(other * f_half, f_half)
         came = w_down.at[origin, pl.ds(row, f_half), h * d_half : (h + 1) * d_half]
@@ -1307,53 +1406,120 @@
             def _():
                 await_bytes(z_more.at[1 + h], came)
 
-        column(origin, h)
+    def next_column(h, side, k):
+        land(h, side, k)
+        column(source(side, k), h)
 
     def next_settle(side, k):
         settle(source(side, k))
 
-    column(s, 0)
-    column(s, 1)
-    advance(29)
-    both_sides(1, functools.partial(next_column, 0))
-    advance(30)
-    both_sides(1, functools.partial(next_column, 1))
-    advance(31)
-    settle(s)
-    advance(32)
-    both_sides(2, functools.partial(next_column, 0))
-    advance(33, 34)
-    both_sides(2, functools.partial(next_column, 1))
-    advance(35)
-    both_sides(1, next_settle)
-    both_sides(3, functools.partial(next_column, 0))
-    both_sides(2, next_settle)
-    for item in pending:
-        item.wait_send()
-
-    @pl.loop(s + 1, n_sp)
-    def _(later):
-        end_copy(later, s).wait_send()
-
-    def sent(side, b):
-        count = max(2, b + 1)
-        for c in range(2):
-            await_bytes(z_send.at[side, c], w_gate.at[: count * k_half, :])
-        await_bytes(z_send.at[side, 2], w_down.at[:count, :f_half, :])
-
-    for side in range(2):
-        for b in range(n_sp - 1):
-            pl.when(behind[side] == b)(functools.partial(sent, side, b))
-
-    def exchanged(count):
-        await_bytes(y_send.at[0], w_gate.at[: count * k_loc, :])
-        await_bytes(y_send.at[1], w_down.at[:count, :f_half, :])
-
-    pl.when(near_end)(functools.partial(exchanged, n_sp - 2))
-    pl.when(jnp.logical_not(near_end))(functools.partial(exchanged, n_sp - 1))
-    both_sides(3, functools.partial(next_column, 1))
-    both_sides(3, next_settle)
-    await_bytes(c_send.at[0], c_in)
+    def next_relay(h, side, k):
+        relay_on(source(side, k), h)
+
+    def columns(k, *parts):
+        for h in parts:
+            both_sides(k, functools.partial(next_column, h))
+
+    def relays(k, *parts):
+        for h in parts:
+            both_sides(k, functools.partial(next_relay, h))
+
+    def far_side(work):
+        for h in range(HALVES):
+            for side in range(2):
+                pl.when(behind[side] > 1)(functools.partial(work, h, side, 1))
+
+    def end_side(work):
+        for h in range(HALVES):
+            for side in range(2):
+                pl.when(behind[side] == 1)(functools.partial(work, h, side, 1))
+
+    def sends_done():
+        for item in pending:
+            item.wait_send()
+
+        @pl.loop(s + 1, n_sp)
+        def _(later):
+            end_copy(later, s).wait_send()
+
+        def sent(side, b):
+            for c, count in ((0, max(2, b + 1)), (1, max(2, b + 1)), (2, max(2, min(b + 1, n_sp - 2)))):
+                await_bytes(z_send.at[side, c], w_gate.at[: count * k_half, :])
+
+        for side in range(2):
+            for b in range(n_sp - 1):
+                pl.when(behind[side] == b)(functools.partial(sent, side, b))
+        await_bytes(y_send.at[1], w_gate.at[: (n_sp - 2) * k_half, :])
+        await_bytes(g_send.at[0], normed.at[0])
+        await_bytes(g_send.at[2], normed.at[0, :e_rows, :])
+
+    @pl.when(end_one)
+    def _():
+        for h in range(HALVES):
+            column(s, h)
+        for h in range(HALVES):
+            relay_on(s, h)
+        advance(29)
+        columns(1, 0)
+        relays(1, 0)
+        advance(30)
+        columns(1, 1)
+        relays(1, 1)
+        advance(31)
+        settle(s)
+        columns(2, 0)
+        relays(2, 0)
+        both_sides(1, next_settle)
+        sends_done()
+        await_bytes(y_send.at[0], w_gate.at[: (n_sp - 1) * k_loc, :])
+        columns(2, 1)
+        relays(2, 1)
+        both_sides(2, next_settle)
+        for h in range(HALVES):
+            back_copy(h).wait_recv()
+            put(taken, h, g_in[h].astype(F32))
+        await_bytes(c_send.at[0], c_in.at[: n_sp - 1])
+
+    @pl.when(inner_one)
+    def _():
+        guest_relay(0)
+        for h in range(HALVES):
+            column(s, h)
+        far_side(next_column)
+        for h in range(HALVES):
+            relay_on(s, h)
+        far_side(next_relay)
+        for h in range(2):
+            guest_tp(h, p, 1, p).wait_recv()
+        gated_half(guest, g_hidden, near_half)
+        guest_relay(1)
+        for h in range(2):
+            guest_tp(h, far, 2, p).wait_recv()
+        gated_half(guest, g_hidden, 1 - near_half)
+        for h in range(HALVES):
+            both_sides(2, functools.partial(land, h))
+        for h in range(HALVES):
+            column(taken, h, g_hidden, n_sp)
+        for h in range(HALVES):
+            relay_on(n_sp, h)
+        end_side(next_column)
+        end_side(next_relay)
+        await_bytes(c_recv.at[n_sp, HALVES], c_in.at[n_sp, :, 1:3])
+        for h in range(HALVES):
+            g_out[h] = total(n_sp, h).astype(BF)
+            back_copy(h).start()
+        for h in range(HALVES):
+            column(taken, h)
+        for h in range(HALVES):
+            relay_on(taken, h)
+        settle(s)
+        both_sides(1, next_settle)
+        sends_done()
+        await_bytes(y_send.at[0], w_gate.at[: (n_sp - 2) * k_loc, :])
+        await_bytes(g_send.at[1], normed.at[0])
+        both_sides(2, next_settle)
+        await_bytes(b_send.at[0], g_out)
+        await_bytes(c_send.at[0], c_in)
 
 
 def quick(
@@ -1432,24 +1598,32 @@
             pltpu.VMEM((own, depth), F32),
             pltpu.VMEM((n_tp, own, depth), BF),
             pltpu.VMEM((n_tp, own, ff), BF),
-            pltpu.VMEM((n_sp, HALVES, n_tp, own, d_half), BF),
-            pltpu.VMEM((n_sp, HALVES, 3, own, d_half), BF),
-            pltpu.VMEM((n_sp, HALVES, own, d_half), BF),
+            pltpu.VMEM((n_sp + 1, HALVES, n_tp, own, d_half), BF),
+            pltpu.VMEM((n_sp + 1, HALVES, 3, own, d_half), BF),
+            pltpu.VMEM((n_sp + 1, HALVES, own, d_half), BF),
+            pltpu.VMEM((n_tp, own, depth), BF),
+            pltpu.VMEM((n_tp, own, ff), BF),
+            pltpu.VMEM((HALVES, own, d_half), BF),
+            pltpu.VMEM((HALVES, own, d_half), BF),
             dma((len(operands),)),
             dma((n_sp,)),
             dma((n_sp,)),
             dma((2, 3)),
-            dma((3, PIECES, n_sp)),
+            dma((3, PIECES, n_sp - 1)),
             dma((2,)),
             dma((1,)),
             dma((n_sp, HALVES)),
             dma((1 + HALVES,)),
+            dma((3,)),
+            dma((4, 2)),
+            dma((1,)),
+            dma((HALVES,)),
             dma((2, 3)),
             dma((2, 3)),
             dma((3,)),
             dma((3,)),
             dma((1,)),
-            dma((n_sp, HALVES + 1)),
+            dma((n_sp + 1, HALVES + 1)),
         ],
         compiler_params=pltpu.CompilerParams(
             collective_id=0, has_side_effects=True, vmem_limit_bytes=60 * 1024 * 1024

time: 95.5 us -> 88 us (0.921)
  Pallas kernels: 94.6 us -> 86.4 us
    pallas_call x1, Pallas kernels: 94.6 us -> 86.4 us  [quick(): pl.pallas_call(functools.partial(quick_kernel, n_sp, width, states), out_...]
where the time goes in v4:
time: 88 us; the launch traced here: 87.2 us
  Pallas kernels  86.4 us (98%)
    pallas_call x1, Pallas kernels, quick(): pl.pallas_call(functools.partial(quick_kernel, n_sp, width, states), out_...  86.4 us

profile of v4, /device:TPU:0, one launch (start us, length us, event | category | flops | bytes accessed | tf_op | source)
XLA Modules:
  0.0 87.2 jit_solution(13520739598364692601)
XLA Ops:
  0.0 86.4 %shard_map.172 = bf16[128,2048]{1,0:T(8,128)(2,1)S(1)} custom-call(bf16[128,2048]{1,0:T(8,128)(2,1)} %residual_h.1, bf16[512,256]{1,0:T(8,128)(2,1)} %u_h.1, bf16[512,512]{1,0:T(8,128)(2,1)} %gate_in_h.1, f32[16,64]{1,0:T(8,128)} %decay_h.1, f32[16,64]{1,0:T(8,128)} %freq_h.1, f32[1,16]{1,0:T(1,128)} %bitcast.17, f32[256,64]{1,0:T(8,128)} %bitcast.11, ...), custom_call_target="tpu_custom_call" | custom-call | tf_op jit(solution)/shard_map/pallas_call | solution.py:1575
  86.4 0.8 copy.20

commit v5 on v4

--- a/solution.py
+++ b/solution.py
@@ -835,6 +835,7 @@
     y_recv,
     y_late,
     z_more,
+    z_last,
     g_send,
     g_recv,
     b_send,
@@ -860,7 +861,7 @@
     n_tp = acts.shape[0]
     k_half, f_half = k_loc // 2, ff // 2
     k_piece, d_half = k_half // PIECES, d_loc // HALVES
-    f_piece = f_half * HALVES // PIECES
+    f_cuts = [f_half * n // PER for n in range(PER + 1)]
 
     barrier = pltpu.get_barrier_semaphore()
     pl.semaphore_signal(barrier, inc=1, device_id={"tp": p})
@@ -910,8 +911,9 @@
         if c < 2:
             row = pl.multiple_of(origin * k_loc + half * k_half + i * k_piece, k_piece)
             return bufs[c].at[pl.ds(row, k_piece), :]
-        row = pl.multiple_of(half * f_half + (i % PER) * f_piece, f_piece)
-        return bufs[c].at[origin, pl.ds(row, f_piece), pl.ds((i // PER) * d_half, d_half)]
+        start, stop = f_cuts[i % PER], f_cuts[i % PER + 1]
+        row = pl.multiple_of(half * f_half + start, 16)
+        return bufs[c].at[origin, pl.ds(row, stop - start), pl.ds((i // PER) * d_half, d_half)]
 
     def z_copy(side, c, i, origin):
         piece = mine(c, i, origin, g)
@@ -943,6 +945,26 @@
             device_id={"sp": ahead(side)},
         )
 
+    def last_copy(side, k):
+        piece = mine(2, PIECES - 1, source(side, k), other)
+        return pltpu.make_async_remote_copy(
+            src_ref=piece,
+            dst_ref=piece,
+            send_sem=z_send.at[side, 2],
+            recv_sem=z_last.at[0],
+            device_id={"sp": ahead(side)},
+        )
+
+    def last_on(side, b):
+        if b > 1:
+            last_copy(side, b - 1).wait_recv()
+        if b < n_sp - 1:
+            last_copy(side, b - 1).start()
+
+    def last_advance(b):
+        for side in range(2):
+            pl.when(behind[side] == b)(functools.partial(last_on, side, b))
+
     def ahead(side):
         return (s + 1) % n_sp if side == 0 else (s + n_sp - 1) % n_sp
 
@@ -1029,7 +1051,11 @@
         if not hold:
             onward(side, k, c, i, last)
 
-        @pl.when(shared(side, k))
+        trade = shared(side, k)
+        if c == 2 and i == PIECES - 1:
+            trade = jnp.logical_and(trade, behind[side] != k + 1)
+
+        @pl.when(trade)
         def _():
             y_copy(c, i, origin, g).start()
 
@@ -1189,7 +1215,7 @@
     loads[9].wait()
 
     def read_block(b):
-        at = pl.ds(pl.multiple_of(b * own, own), own)
+        at = pl.ds(pl.multiple_of(b * 2 * own, own), 2 * own)
         high, small = split(st_real[at, :])
         y = mm_t(high, wide[4]) + mm_t(small, wide[4]) + mm_t(high, wide[5])
         high, small = split(st_imag[at, :])
@@ -1197,10 +1223,10 @@
         y = y + skip[...] * u[at, :].astype(F32)
         acts[t, at, :] = jax.nn.gelu(y).astype(BF)
 
-    half_rows = rows // own // 2
+    half_rows = rows // own // 4
     pl.loop(0, half_rows)(read_block)
     advance(6)
-    pl.loop(half_rows, rows // own)(read_block)
+    pl.loop(half_rows, rows // own // 2)(read_block)
     advance(7)
 
     def gather_tp(buf, lane_no, between, later):
@@ -1297,6 +1323,7 @@
 
     def while_gathering():
         advance(18, 19)
+        last_advance(1)
         pl.when(inner_one)(inner_first)
         advance(20, 21, 22)
         pl.when(inner_one)(lambda: guest_take(0))
@@ -1315,6 +1342,8 @@
             def _():
                 for i in range(PIECES):
                     more_copy(side, 2, i).start()
+
+    last_advance(2)
 
     @pl.when(inner_one)
     def _():
@@ -1354,9 +1383,10 @@
     def column(o, h, rows_in=hidden, slot=None):
         slot = o if slot is None else slot
         weight = w_down.at[o, :, h * d_half : (h + 1) * d_half]
-        product = mm(rows_in[...].reshape(n_tp * own, ff), weight[...]).astype(BF)
-        c_part[slot, h] = product.reshape(n_tp, own, d_half)
-        for index in range(2):
+        for index, b in enumerate((1 - near_half, near_half)):
+            some = pl.ds(b * duo, duo)
+            product = mm(rows_in[some].reshape(duo * own, ff), weight[...]).astype(BF)
+            c_part[slot, h, some] = product.reshape(duo, own, d_half)
             col_pair(slot, h, index).start()
 
     def relay_on(o, h):
@@ -1396,7 +1426,15 @@
         row = pl.multiple_of(other * f_half, f_half)
         came = w_down.at[origin, pl.ds(row, f_half), h * d_half : (h + 1) * d_half]
 
-        @pl.when(shared(side, k))
+        whole = shared(side, k)
+        if h == HALVES - 1:
+            whole = jnp.logical_and(whole, behind[side] != k + 1)
+
+            @pl.when(behind[side] == k + 1)
+            def _():
+                await_bytes(y_late.at[origin, h], mine(2, h * PER, origin, other))
+
+        @pl.when(whole)
         def _():
             await_bytes(y_late.at[origin, h], came)
 
@@ -1443,13 +1481,15 @@
             end_copy(later, s).wait_send()
 
         def sent(side, b):
-            for c, count in ((0, max(2, b + 1)), (1, max(2, b + 1)), (2, max(2, min(b + 1, n_sp - 2)))):
-                await_bytes(z_send.at[side, c], w_gate.at[: count * k_half, :])
+            early, late = max(2, b + 1), max(2, min(b + 1, n_sp - 2))
+            tail = k_piece if b > 0 else 0
+            for c, size in enumerate((early * k_half, early * k_half, late * k_half + tail)):
+                await_bytes(z_send.at[side, c], w_gate.at[:size, :])
 
         for side in range(2):
             for b in range(n_sp - 1):
                 pl.when(behind[side] == b)(functools.partial(sent, side, b))
-        await_bytes(y_send.at[1], w_gate.at[: (n_sp - 2) * k_half, :])
+        await_bytes(y_send.at[1], w_gate.at[: (n_sp - 2) * k_half - k_piece, :])
         await_bytes(g_send.at[0], normed.at[0])
         await_bytes(g_send.at[2], normed.at[0, :e_rows, :])
 
@@ -1472,6 +1512,7 @@
         both_sides(1, next_settle)
         sends_done()
         await_bytes(y_send.at[0], w_gate.at[: (n_sp - 1) * k_loc, :])
+        last_advance(n_sp - 1)
         columns(2, 1)
         relays(2, 1)
         both_sides(2, next_settle)
@@ -1482,13 +1523,13 @@
 
     @pl.when(inner_one)
     def _():
-        guest_relay(0)
         for h in range(HALVES):
             column(s, h)
         far_side(next_column)
         for h in range(HALVES):
             relay_on(s, h)
         far_side(next_relay)
+        guest_relay(0)
         for h in range(2):
             guest_tp(h, p, 1, p).wait_recv()
         gated_half(guest, g_hidden, near_half)
@@ -1503,15 +1544,15 @@
         for h in range(HALVES):
             relay_on(n_sp, h)
         end_side(next_column)
+        for h in range(HALVES):
+            column(taken, h)
         end_side(next_relay)
+        for h in range(HALVES):
+            relay_on(taken, h)
         await_bytes(c_recv.at[n_sp, HALVES], c_in.at[n_sp, :, 1:3])
         for h in range(HALVES):
             g_out[h] = total(n_sp, h).astype(BF)
             back_copy(h).start()
-        for h in range(HALVES):
-            column(taken, h)
-        for h in range(HALVES):
-            relay_on(taken, h)
         settle(s)
         both_sides(1, next_settle)
         sends_done()
@@ -1614,6 +1655,7 @@
             dma((1,)),
             dma((n_sp, HALVES)),
             dma((1 + HALVES,)),
+            dma((1,)),
             dma((3,)),
             dma((4, 2)),
             dma((1,)),

time: 88 us -> 86.5 us (0.983)
  Pallas kernels: 86.4 us -> 85.5 us
where the time goes in v5:
time: 86.5 us; the launch traced here: 86.4 us
  Pallas kernels  85.5 us (99%)
    pallas_call x1, Pallas kernels, quick(): pl.pallas_call(functools.partial(quick_kernel, n_sp, width, states), out_...  85.5 us

profile of v5, /device:TPU:0, one launch (start us, length us, event | category | flops | bytes accessed | tf_op | source)
XLA Modules:
  0.0 86.4 jit_solution(3680200539773082230)
XLA Ops:
  0.0 85.5 %shard_map.172 = bf16[128,2048]{1,0:T(8,128)(2,1)S(1)} custom-call(bf16[128,2048]{1,0:T(8,128)(2,1)} %residual_h.1, bf16[512,256]{1,0:T(8,128)(2,1)} %u_h.1, bf16[512,512]{1,0:T(8,128)(2,1)} %gate_in_h.1, f32[16,64]{1,0:T(8,128)} %decay_h.1, f32[16,64]{1,0:T(8,128)} %freq_h.1, f32[1,16]{1,0:T(1,128)} %bitcast.17, f32[256,64]{1,0:T(8,128)} %bitcast.11, ...), custom_call_target="tpu_custom_call" | custom-call | tf_op jit(solution)/shard_map/pallas_call | solution.py:1616
  85.6 0.8 copy.20

commit v6 on v5

--- a/solution.py
+++ b/solution.py
@@ -1123,9 +1123,9 @@
             for j, piece in enumerate(split(kept)):
                 wide[2 * i + j, :, at] = piece
 
-    @pl.loop(0, rows // own)
+    @pl.loop(0, rows // own // 2)
     def _(b):
-        at = pl.ds(pl.multiple_of(b * own, own), own)
+        at = pl.ds(pl.multiple_of(b * 2 * own, own), 2 * own)
         x = u[at, :]
         push_re = mm(x, wide[0]) + mm(x, wide[1])
         push_im = mm(x, wide[2]) + mm(x, wide[3])

time: 86.5 us -> 86.5 us (level)
  no operation moved by 1% of the time
where the time goes in v6:
time: 86.5 us; the launch traced here: 86.4 us
  Pallas kernels  85.5 us (99%)
    pallas_call x1, Pallas kernels, quick(): pl.pallas_call(functools.partial(quick_kernel, n_sp, width, states), out_...  85.5 us

profile of v6, /device:TPU:0, one launch (start us, length us, event | category | flops | bytes accessed | tf_op | source)
XLA Modules:
  0.0 86.4 jit_solution(11616040444980693209)
XLA Ops:
  0.0 85.5 %shard_map.172 = bf16[128,2048]{1,0:T(8,128)(2,1)S(1)} custom-call(bf16[128,2048]{1,0:T(8,128)(2,1)} %residual_h.1, bf16[512,256]{1,0:T(8,128)(2,1)} %u_h.1, bf16[512,512]{1,0:T(8,128)(2,1)} %gate_in_h.1, f32[16,64]{1,0:T(8,128)} %decay_h.1, f32[16,64]{1,0:T(8,128)} %freq_h.1, f32[1,16]{1,0:T(1,128)} %bitcast.17, f32[256,64]{1,0:T(8,128)} %bitcast.11, ...), custom_call_target="tpu_custom_call" | custom-call | tf_op jit(solution)/shard_map/pallas_call | solution.py:1616
  85.6 0.8 copy.20
